TPU v7x, 32 devices: a whole 2x2x4 slice. The times are simulated.
32 devices in a mesh: ep: 8 (over z, x), tp: 4 (over y, core).
Axes of the slice: x: 2, y: 2, z: 4, core: 2. Of those that a mesh axis runs over, the one named last changes fastest.
Arguments:
- queries: bfloat16 [2048, 4096], P('ep', 'tp'), may hold values from -6 to 6
- key_rows: bfloat16 [2048, 4096], P('ep', 'tp'), may hold values from -6 to 6
- value_rows: bfloat16 [2048, 4096], P('ep', 'tp'), may hold values from -6 to 6
- lambdas: float32 [16], P('tp'), may hold values from 0.3 to 0.8
- head_gain: float32 [256], replicated, may hold values from 0.1 to 1.9
- out_proj: bfloat16 [4096, 2048], P('tp'), may hold values from -0.09375 to 0.09375
- moe_input: bfloat16 [1024, 2048], P('ep'), may hold values from -6 to 6
- moe_gain: float32 [2048], replicated, may hold values from 0.1 to 1.9
- routes: int32 [1024, 2], P('ep'), may hold values from 0 to 7, all different within a row; in each aligned block of 32 rows (0 to 31, 32 to 63, ...) at most 16 rows name the same one
- route_weights: float32 [1024, 2], P('ep'), may hold values from 0.2 to 1.2
- expert_gate: bfloat16 [8, 2048, 1024], P('ep', None, 'tp'), may hold values from -0.125 to 0.125
- expert_up: bfloat16 [8, 2048, 1024], P('ep', None, 'tp'), may hold values from -0.125 to 0.125
- expert_down: bfloat16 [8, 1024, 2048], P('ep', 'tp'), may hold values from -0.1875 to 0.1875
- shared_gate: bfloat16 [2048, 1024], P(None, 'tp'), may hold values from -0.125 to 0.125
- shared_up: bfloat16 [2048, 1024], P(None, 'tp'), may hold values from -0.125 to 0.125
- shared_down: bfloat16 [1024, 2048], P('tp'), may hold values from -0.1875 to 0.1875
Outputs:
- mixer_out: bfloat16 [2048, 2048], P(('ep', 'tp'))
- moe_out: bfloat16 [1024, 2048], P(('ep', 'tp'))
Inputs may be any that keep to these rules, and one draw needn't show every extreme that they name: `routes`: each row names 2 different experts. The rows of one index of ep fall into 4 aligned blocks of equal size; no expert is named by more than 16 rows of one block, and in every draw some expert is named by exactly 16 rows of some block.
All inputs are finite; a program needn't handle non-finite values.
Results may differ from a plain program's by a relative error of at most 0.02.
Values may be sent and summed in bfloat16 or wider, within the bound.
A program may use at most 128 MiB of HBM per device.

v0:
```python
import functools
import jax
import jax.numpy as jnp
from jax import lax
from jax.experimental import pallas as pl
from jax.experimental.pallas import tpu as pltpu
from jax.sharding import PartitionSpec as P

theta_base = 500000.0
norm_eps = 1e-06
head_eps = 1e-05
MESH = pl.DeviceIdType.MESH
log2_e = 1.4426950408889634


def rotate(matrix, positions, head_dim):
    row_count = matrix.shape[0]
    shaped = matrix.reshape(row_count, -1, head_dim).astype(jnp.float32)
    half_dim = head_dim // 2
    frequency = jnp.power(theta_base, -jnp.arange(half_dim, dtype=jnp.float32) * 2.0 / head_dim)
    angles = positions.astype(jnp.float32)[:, None] * frequency[None, :]
    cosine = jnp.cos(angles)[:, None, :]
    sines = jnp.sin(angles)[:, None, :]
    front_half = shaped[..., :half_dim]
    second = shaped[..., half_dim:]
    turned = jnp.concatenate(
        [front_half * cosine - second * sines, second * cosine + front_half * sines], axis=-1
    )
    return turned.reshape(matrix.shape).astype(jnp.bfloat16)


def rms_rows(values, gain):
    widened = values.astype(jnp.float32)
    mean_square = jnp.mean(widened * widened, axis=-1, keepdims=True)
    return (widened * lax.rsqrt(mean_square + norm_eps) * gain).astype(jnp.bfloat16)


def gated_hidden(rows_in, gate_weight, up_weight):
    gate_part = jnp.dot(rows_in, gate_weight, preferred_element_type=jnp.float32)
    up_part = jnp.dot(rows_in, up_weight, preferred_element_type=jnp.float32)
    return (jax.nn.silu(gate_part) * up_part).astype(jnp.bfloat16)


def slot_hidden(slot_rows, gate_weight, up_weight):
    gate_part = jnp.einsum(
        "xnsd,xdf->xnsf", slot_rows, gate_weight, preferred_element_type=jnp.float32
    )
    up_part = jnp.einsum("xnsd,xdf->xnsf", slot_rows, up_weight, preferred_element_type=jnp.float32)
    return (jax.nn.silu(gate_part) * up_part).astype(jnp.bfloat16)


def key_block_size(piece_rows):
    for candidate in (1024, 512):
        return candidate
    return piece_rows


def fold_keys(state_in, pieces, rot_query, head_count, head_dim):
    keys_piece, values_piece = pieces
    piece_rows = keys_piece.shape[0]
    block_rows = key_block_size(piece_rows)
    block_count = piece_rows // block_rows
    query_view = rot_query.reshape(rot_query.shape[0], head_count, 2, head_dim)
    score_scale = head_dim ** (-0.5)

    def one_block(running, key_block):
        running_max, denominator, numerator = running
        key_view = key_block[0].reshape(block_rows, head_count, 2, head_dim)
        value_view = key_block[1].reshape(block_rows, head_count, 2 * head_dim)
        scores = (
            jnp.einsum("qhmd,khmd->hmqk", query_view, key_view, preferred_element_type=jnp.float32)
            * score_scale
        )
        newest = jnp.maximum(running_max, jnp.max(scores, axis=-1))
        weights = jnp.exp(scores - newest[..., None])
        shrink = jnp.exp(running_max - newest)
        denominator = denominator * shrink + jnp.sum(weights, axis=-1)
        weighted = jnp.einsum(
            "hmqk,khe->hmqe",
            weights.astype(jnp.bfloat16),
            value_view,
            preferred_element_type=jnp.float32,
        )
        numerator = numerator * shrink[..., None] + weighted
        return ((newest, denominator, numerator), None)

    blocks = (
        keys_piece.reshape(block_count, block_rows, -1),
        values_piece.reshape(block_count, block_rows, -1),
    )
    result, _ = lax.scan(one_block, state_in, blocks)
    return result


def slot_table(route_block, expert_count, capacity):
    flat_routes = route_block.reshape(-1)
    route_total = flat_routes.shape[0]
    top_count = route_block.shape[1]
    experts_iota = jnp.arange(expert_count, dtype=jnp.int32)
    onehot = (flat_routes[:, None] == experts_iota[None, :]).astype(jnp.int32)
    before = jnp.cumsum(onehot, axis=0) - onehot
    slot_rank = jnp.sum(before * onehot, axis=1)
    slot_iota = jnp.arange(capacity, dtype=jnp.int32)
    matches = (flat_routes[None, None, :] == experts_iota[:, None, None]) & (
        slot_rank[None, None, :] == slot_iota[None, :, None]
    )
    source_row = jnp.arange(route_total, dtype=jnp.int32) // top_count
    source = jnp.sum(jnp.where(matches, source_row[None, None, :], 0), axis=2)
    filled = jnp.any(matches, axis=2)
    return (source, filled, slot_rank.reshape(route_block.shape))


def fill_slots(rows_src, source, filled):
    taken = jnp.take(rows_src, source.reshape(-1), axis=0).reshape(
        source.shape + (rows_src.shape[1],)
    )
    return jnp.where(filled[..., None], taken, jnp.zeros_like(taken))


def rotation_tables(positions, head_dim):
    half_dim = head_dim // 2
    frequency = jnp.power(theta_base, -jnp.arange(half_dim, dtype=jnp.float32) * 2.0 / head_dim)
    angles = positions.astype(jnp.float32)[:, None] * frequency[None, :]
    cosine, sines = jnp.cos(angles), jnp.sin(angles)
    return (
        jnp.concatenate([cosine, cosine], axis=1),
        jnp.concatenate([-sines, sines], axis=1),
    )


def prepare_kernel(
    expert_count, capacity, rows_ref, gain_ref, routes_ref, scale_ref, norm_ref, out_ref, mix_ref
):
    own_rows = mix_ref.shape[0]
    slots = expert_count * capacity
    widened = rows_ref[...].astype(jnp.float32)
    mean_square = jnp.mean(widened * widened, axis=-1, keepdims=True)
    norm_ref[...] = (widened * lax.rsqrt(mean_square + norm_eps) * gain_ref[...]).astype(
        jnp.bfloat16
    )
    own = pl.ds(pl.multiple_of(lax.axis_index("tp") * own_rows, own_rows), own_rows)
    routes = routes_ref[own, :]
    scales = scale_ref[own, :]
    lane = lax.broadcasted_iota(jnp.int32, (own_rows, slots), 1)
    lane_expert, lane_slot = lane // capacity, lax.rem(lane, capacity)
    hits = [routes[:, k : k + 1] == lane_expert for k in range(routes.shape[1])]
    named = sum(hit.astype(jnp.float32) for hit in hits).astype(jnp.bfloat16)
    row_at = lax.broadcasted_iota(jnp.int32, (own_rows, own_rows), 0)
    other_at = lax.broadcasted_iota(jnp.int32, (own_rows, own_rows), 1)
    earlier = (other_at < row_at).astype(jnp.float32).astype(jnp.bfloat16)
    before = jnp.dot(earlier, named, preferred_element_type=jnp.float32).astype(jnp.int32)
    chosen = [jnp.logical_and(hit, before == lane_slot).astype(jnp.float32) for hit in hits]
    mix_ref[...] = sum(scales[:, k : k + 1] * chosen[k] for k in range(len(chosen)))
    out_ref[...] = lax.dot_general(
        sum(chosen).astype(jnp.bfloat16),
        norm_ref[own, :],
        (((0,), (0,)), ((), ())),
        preferred_element_type=jnp.float32,
    ).astype(jnp.bfloat16)


def prepare(moe_input, moe_gain, routes, route_weights, tp_count, expert_count, capacity):
    rows, model = moe_input.shape
    slots = expert_count * capacity
    return pl.pallas_call(
        functools.partial(prepare_kernel, expert_count, capacity),
        out_shape=(
            jax.ShapeDtypeStruct((rows, model), jnp.bfloat16),
            jax.ShapeDtypeStruct((slots, model), jnp.bfloat16),
            jax.ShapeDtypeStruct((rows // tp_count, slots), jnp.float32),
        ),
        name="prepare",
    )(moe_input, moe_gain[None, :], routes, route_weights)


def mixer_kernel(
    ep_count,
    tp_count,
    cos_ref,
    sin_ref,
    lam_ref,
    gain_ref,
    norm_ref,
    slot_ref,
    mix_ref,
    q_hbm,
    k_hbm,
    v_hbm,
    proj_hbm,
    gate_hbm,
    up_hbm,
    down_hbm,
    sgate_hbm,
    sup_hbm,
    sdown_hbm,
    out_ref,
    moe_ref,
    raw,
    pack_ref,
    q_sem,
    proj_ref,
    gate_ref,
    up_ref,
    down_ref,
    sgate_ref,
    sup_ref,
    sdown_ref,
    xbuf,
    hidden,
    pair_out,
    pair_own,
    pair_in,
    far_in,
    shared_sum,
    ret_out,
    ret_in,
    w_sem,
    d_send,
    d_recv,
    g_send,
    g_recv,
    h_send,
    h_recv,
    p_sem,
    y_send,
    y_recv,
    v_send,
    v_recv,
    qbuf,
    kbuf,
    vbuf,
    lam_other,
    obuf,
    heads,
    sum_out,
    sum_in,
    block_out,
    block_in,
    s_send,
    s_recv,
    s_local,
    f_send,
    f_recv,
    l_sem,
    o_send,
    o_recv,
    r_send,
    r_recv,
    b_send,
    b_recv,
):
    head_count = pack_ref.shape[1]
    half, width = pack_ref.shape[3], pack_ref.shape[4]
    head_dim = width // 2
    e = lax.axis_index("ep")
    t = lax.axis_index("tp")
    y, c = t // 2, lax.rem(t, 2)
    partner = y * 2 + 1 - c
    s_me, h_me = e // head_count, lax.rem(e, head_count)
    y_count = tp_count // 2

    def remote(src, dst, send, recv, where):
        return pltpu.make_async_remote_copy(
            src_ref=src,
            dst_ref=dst,
            send_sem=send,
            recv_sem=recv,
            device_id=where,
            device_id_type=MESH,
        )

    def landing(which, side, source):
        if which == 0:
            return qbuf.at[pl.ds(source * half, half)]
        return (kbuf, vbuf)[which - 1].at[pl.ds((side * ep_count + source) * half, half)]

    def first_copy(which, h, side):
        return remote(
            pack_ref.at[which, h, side],
            landing(which, side, e),
            s_send.at[which, h, side],
            s_recv.at[which, e],
            (c * head_count + h, y * 2 + side),
        )

    def own_copy(which):
        return pltpu.make_async_copy(
            pack_ref.at[which, h_me, c], landing(which, c, e), s_local.at[which]
        )

    def forward(which, source):
        place = landing(which, c, source)
        return remote(
            place, place, f_send.at[which - 1, source], f_recv.at[which - 1, source], (e, partner)
        )

    raw_copies = [
        pltpu.make_async_copy(ref, raw.at[at], q_sem.at[at])
        for at, ref in enumerate((q_hbm, k_hbm, v_hbm))
    ]
    for copy in raw_copies:
        copy.start()
    weight_copies = [
        pltpu.make_async_copy(a, b, w_sem.at[at])
        for at, (a, b) in enumerate(
            (
                (sgate_hbm, sgate_ref),
                (sup_hbm, sup_ref),
                (sdown_hbm, sdown_ref),
                (gate_hbm.at[0], gate_ref),
                (up_hbm.at[0], up_ref),
                (down_hbm.at[0], down_ref),
                (proj_hbm, proj_ref),
            )
        )
    ]
    for copy in weight_copies:
        copy.start()

    capacity = xbuf.shape[2]
    own_rows = moe_ref.shape[0]
    slots = ep_count * capacity

    def dispatch(target):
        rows = pl.ds(pl.multiple_of(target * capacity, capacity), capacity)
        return remote(
            slot_ref.at[rows], xbuf.at[t, e], d_send.at[target], d_recv.at[e], (target, t)
        )

    own_slots = pl.ds(pl.multiple_of(e * capacity, capacity), capacity)
    own_dispatch = pltpu.make_async_copy(slot_ref.at[own_slots], xbuf.at[t, e], d_recv.at[e])
    own_dispatch.start()

    def start_dispatch(j, carry):
        dispatch(lax.rem(e + 1 + j, ep_count)).start()
        return carry

    lax.fori_loop(0, ep_count - 1, start_dispatch, 0)

    lam_copy = remote(lam_ref, lam_other, l_sem.at[0], l_sem.at[1], (e, partner))
    lam_copy.start()

    mine = s_me == c

    def each_send(act):
        def body(j, carry):
            h = lax.rem(h_me + 1 + j, head_count)
            for k in range(2):
                side = lax.rem(c + 1 + k, 2)
                own = jnp.logical_and(c * head_count + h == e, side == c)
                act(h, side, own)
            return carry

        lax.fori_loop(0, head_count, body, 0)

    def start_send(h, side, own):
        @pl.when(jnp.logical_not(own))
        def _():
            for which in range(3):
                first_copy(which, h, side).start()

        @pl.when(own)
        def _():
            for which in range(3):
                own_copy(which).start()

    for copy in raw_copies:
        copy.wait()

    def pack_head(h):
        cosine = cos_ref[...]
        sines = sin_ref[...]
        for which in range(2):
            for m in range(2):
                at = pl.multiple_of(h * width + m * head_dim, head_dim)
                part = raw[which, :, pl.ds(at, head_dim)].astype(jnp.float32)
                turned = part * cosine + pltpu.roll(part, head_dim // 2, 1) * sines
                turned = turned.astype(jnp.bfloat16)
                for side in range(2):
                    pack_ref[which, h, side, :, m * head_dim : (m + 1) * head_dim] = turned[
                        side * half : (side + 1) * half
                    ]
        at = pl.multiple_of(h * width, width)
        for side in range(2):
            pack_ref[2, h, side] = raw[2, side * half : (side + 1) * half, pl.ds(at, width)]

    def head_at(j):
        return lax.rem(h_me + 1 + j, head_count)

    def send_head(h):
        for k in range(2):
            side = lax.rem(c + 1 + k, 2)
            start_send(h, side, jnp.logical_and(c * head_count + h == e, side == c))

    pack_head(head_at(0))

    def pack_and_send(j, carry):
        pack_head(head_at(j))
        send_head(head_at(j - 1))
        return carry

    lax.fori_loop(1, head_count, pack_and_send, 0)
    send_head(head_at(head_count - 1))

    for copy in weight_copies[:3]:
        copy.wait()
    normed = norm_ref[...]
    gate_part = jnp.dot(normed, sgate_ref[...], preferred_element_type=jnp.float32)
    up_part = jnp.dot(normed, sup_ref[...], preferred_element_type=jnp.float32)
    shared_hidden = (gate_part / (1.0 + jnp.exp(-gate_part)) * up_part).astype(jnp.bfloat16)
    shared_part = jnp.dot(
        shared_hidden, sdown_ref[...], preferred_element_type=jnp.float32
    ).astype(jnp.bfloat16)
    for v in range(y_count):
        for core in range(2):
            block = shared_part[(v * 2 + core) * own_rows : (v * 2 + core + 1) * own_rows]

            @pl.when(c == core)
            def _():
                pair_own[v, :own_rows, :] = block

            @pl.when(c != core)
            def _():
                pair_out[v, :own_rows, :] = block

    def spread(place, source, far):
        if far == 0:
            sends, recvs, where = g_send.at[source, 0], g_recv.at[source, 0], (e, partner)
        else:
            there = lax.rem(y + far, y_count)
            sends, recvs = g_send.at[source, far], g_recv.at[source, far]
            where = (e, there * 2 + c)
        return remote(place, place, sends, recvs, where)

    def arrive_slots(j, carry):
        source = lax.rem(e + j, ep_count)
        place = xbuf.at[t, source]

        @pl.when(source == e)
        def _():
            own_dispatch.wait()

        @pl.when(source != e)
        def _():
            remote(
                place, place, d_send.at[source], d_recv.at[source], (e, partner)
            ).wait_recv()

        for far in range(1, y_count):
            spread(place, source, far).start()
        spread(place, source, 0).start()
        return carry

    lax.fori_loop(0, ep_count, arrive_slots, 0)

    def relay(source, far, core):
        from_y = lax.rem(y + y_count - far, y_count)
        place = xbuf.at[from_y * 2 + core, source]
        return remote(
            place, place, h_send.at[source, far - 1], h_recv.at[source, far - 1], (e, partner)
        )

    def arrive_far(j, carry):
        source = lax.rem(e + j, ep_count)
        for far in range(1, y_count):
            from_y = lax.rem(y + y_count - far, y_count)
            spread(xbuf.at[from_y * 2 + c, source], source, far).wait_recv()
            relay(source, far, c).start()
        return carry

    lax.fori_loop(0, ep_count, arrive_far, 0)

    def arrive_relay(j, carry):
        source = lax.rem(e + j, ep_count)
        spread(xbuf.at[partner, source], source, 0).wait_recv()
        for far in range(1, y_count):
            relay(source, far, 1 - c).wait_recv()
        return carry

    lax.fori_loop(0, ep_count, arrive_relay, 0)

    for copy in weight_copies[3:6]:
        copy.wait()
    rows_in = xbuf[...].reshape(tp_count * slots, xbuf.shape[3])
    gate_part = jnp.dot(rows_in, gate_ref[...], preferred_element_type=jnp.float32)
    up_part = jnp.dot(rows_in, up_ref[...], preferred_element_type=jnp.float32)
    hidden[...] = (
        (gate_part / (1.0 + jnp.exp(-gate_part)) * up_part).astype(jnp.bfloat16)
    ).reshape(hidden.shape)

    def down_part(core, into):
        rows = jnp.concatenate([hidden[v * 2 + core] for v in range(y_count)], axis=0)
        product = jnp.dot(rows, down_ref[...], preferred_element_type=jnp.float32)
        product = product.astype(jnp.bfloat16)
        for v in range(y_count):
            into[v, own_rows:, :] = product[v * slots : (v + 1) * slots]

    down_part(1 - c, pair_out)
    near_copy = remote(pair_out, pair_in, p_sem.at[0], p_sem.at[1], (e, partner))
    near_copy.start()
    down_part(c, pair_own)
    near_copy.wait()
    pair_own[...] = (
        pair_own[...].astype(jnp.float32) + pair_in[...].astype(jnp.float32)
    ).astype(jnp.bfloat16)

    def far_copy(step):
        target = lax.rem(y + step, y_count)
        return remote(
            pair_own.at[target],
            far_in.at[step - 1],
            y_send.at[step - 1],
            y_recv.at[step - 1],
            (e, target * 2 + c),
        )

    for step in range(1, y_count):
        far_copy(step).start()
    def arrive(j, carry):
        source = lax.rem(e + j, ep_count)
        own = jnp.logical_and(source == e, mine)
        for which in range(3):

            @pl.when(own)
            def _():
                own_copy(which).wait()

            @pl.when(jnp.logical_not(own))
            def _():
                place = landing(which, c, source)
                remote(
                    place, place, f_send.at[0, source], s_recv.at[which, source], (e, partner)
                ).wait_recv()

            if which > 0:
                forward(which, source).start()
        return carry

    lax.fori_loop(0, ep_count, arrive, 0)

    for step in range(1, y_count):
        far_copy(step).wait_recv()
    expert_sum = pair_own[y].astype(jnp.float32)
    for step in range(1, y_count):
        expert_sum = expert_sum + far_in[step - 1].astype(jnp.float32)
    shared_sum[...] = expert_sum[:own_rows]
    ret_out[...] = expert_sum[own_rows:].astype(jnp.bfloat16).reshape(ret_out.shape)

    def give_back(target):
        return remote(
            ret_out.at[target], ret_in.at[e], v_send.at[target], v_recv.at[e], (target, t)
        )

    own_back = pltpu.make_async_copy(ret_out.at[e], ret_in.at[e], v_recv.at[e])
    own_back.start()

    def start_back(j, carry):
        give_back(lax.rem(e + 1 + j, ep_count)).start()
        return carry

    lax.fori_loop(0, ep_count - 1, start_back, 0)

    def arrive_forward(j, carry):
        source = lax.rem(e + j, ep_count)
        for which in (1, 2):
            place = landing(which, 1 - c, source)
            remote(
                place,
                place,
                f_send.at[which - 1, source],
                f_recv.at[which - 1, source],
                (e, partner),
            ).wait_recv()
        return carry

    lax.fori_loop(0, ep_count, arrive_forward, 0)
    lam_copy.wait()

    lam = jnp.where(mine, lam_ref[h_me], lam_other[h_me])[0:1, 0:1]
    gain = gain_ref[...]
    factor = head_dim ** (-0.5) * log2_e

    def back_copy(target):
        return remote(
            obuf.at[target],
            heads.at[h_me, pl.ds(c * half, half)],
            o_send.at[target],
            o_recv.at[h_me, c],
            (target, y * 2 + s_me),
        )

    def back_own():
        return pltpu.make_async_copy(
            obuf.at[e], heads.at[h_me, pl.ds(c * half, half)], o_recv.at[h_me, c]
        )

    def attend(j, carry):
        target = lax.rem(e + 1 + j, ep_count)
        block = qbuf[pl.ds(target * half, half), :]
        ratios = []
        for m in range(2):
            columns = slice(m * head_dim, (m + 1) * head_dim)
            scores = lax.dot_general(
                block[:, columns],
                kbuf[:, columns],
                (((1,), (1,)), ((), ())),
                preferred_element_type=jnp.float32,
            )
            top = jnp.max(scores, axis=-1, keepdims=True)
            weights = jnp.exp2((scores - top) * factor)
            denominator = jnp.sum(weights, axis=-1, keepdims=True)
            weighted = jnp.dot(
                weights.astype(jnp.bfloat16), vbuf[...], preferred_element_type=jnp.float32
            )
            ratios.append(weighted / denominator)
        mixed = ratios[0] - lam * ratios[1]
        mean_square = jnp.mean(mixed * mixed, axis=-1, keepdims=True)
        obuf[target] = (mixed * lax.rsqrt(mean_square + head_eps) * gain).astype(jnp.bfloat16)
        own = jnp.logical_and(target == e, mine)

        @pl.when(jnp.logical_not(own))
        def _():
            back_copy(target).start()

        @pl.when(own)
        def _():
            back_own().start()

        return carry

    lax.fori_loop(0, ep_count, attend, 0)

    own_back.wait()

    def arrive_back(j, carry):
        source = lax.rem(e + 1 + j, ep_count)
        place = ret_in.at[source]
        remote(place, place, v_send.at[source], v_recv.at[source], (e, partner)).wait_recv()
        return carry

    lax.fori_loop(0, ep_count - 1, arrive_back, 0)
    mix = mix_ref[...]
    coarse = mix.astype(jnp.bfloat16)
    fine = (mix - coarse.astype(jnp.float32)).astype(jnp.bfloat16)
    returned = ret_in[...].reshape(slots, ret_in.shape[2])
    combined = jnp.dot(coarse, returned, preferred_element_type=jnp.float32)
    combined = combined + jnp.dot(fine, returned, preferred_element_type=jnp.float32)
    moe_ref[...] = (shared_sum[...] + combined).astype(jnp.bfloat16)

    def arrive_heads(h, carry):
        for side in range(2):
            own = jnp.logical_and(c * head_count + h == e, side == c)
            place = heads.at[h, pl.ds(side * half, half)]

            @pl.when(own)
            def _():
                back_own().wait()

            @pl.when(jnp.logical_not(own))
            def _():
                remote(
                    place, place, o_send.at[0], o_recv.at[h, side], (e, partner)
                ).wait_recv()

        return carry

    lax.fori_loop(0, head_count, arrive_heads, 0)

    weight_copies[6].wait()
    share = out_ref.shape[0]

    def partial(core):
        total = None
        for h in range(head_count):
            rows = jnp.concatenate(
                [heads[h, pl.ds((v * 2 + core) * share, share), :] for v in range(y_count)], axis=0
            )
            term = jnp.dot(
                rows,
                proj_ref[h * width : (h + 1) * width, :],
                preferred_element_type=jnp.float32,
            )
            total = term if total is None else total + term
        return total.astype(jnp.bfloat16)

    sum_out[...] = partial(1 - c)
    pair_copy = remote(sum_out, sum_in, r_send.at[0], r_recv.at[0], (e, partner))
    pair_copy.start()
    kept = partial(c).astype(jnp.float32)
    pair_copy.wait()
    block_out[...] = (
        (kept + sum_in[...].astype(jnp.float32)).astype(jnp.bfloat16).reshape(block_out.shape)
    )

    def block_copy(step):
        target = lax.rem(y + step, y_count)
        return remote(
            block_out.at[target],
            block_in.at[step - 1],
            b_send.at[step - 1],
            b_recv.at[step - 1],
            (e, target * 2 + c),
        )

    for step in range(1, y_count):
        block_copy(step).start()
    total = block_out[y].astype(jnp.float32)
    for step in range(1, y_count):
        block_copy(step).wait()
        total = total + block_in[step - 1].astype(jnp.float32)
    out_ref[...] = total.astype(jnp.bfloat16)

    def end_send(h, side, own):
        @pl.when(jnp.logical_not(own))
        def _():
            for which in range(3):
                first_copy(which, h, side).wait_send()

    each_send(end_send)

    for step in range(1, y_count):
        far_copy(step).wait_send()

    def end_rest(source, carry):
        for far in range(y_count):
            spread(xbuf.at[t, source], source, far).wait_send()
        for far in range(1, y_count):
            relay(source, far, c).wait_send()

        @pl.when(source != e)
        def _():
            dispatch(source).wait_send()
            give_back(source).wait_send()

        for which in (1, 2):
            forward(which, source).wait_send()

        @pl.when(jnp.logical_not(jnp.logical_and(source == e, mine)))
        def _():
            back_copy(source).wait_send()

        return carry

    lax.fori_loop(0, ep_count, end_rest, 0)


def mixer(
    tables, sequence, lambdas, head_gain, out_proj, prepared, expert_weights, ep_count, tp_count
):
    normed, outgoing, mixing = prepared
    head_count = lambdas.shape[0]
    half = sequence[0].shape[0] // 2
    width = sequence[0].shape[1] // head_count
    slots = outgoing.shape[0]
    capacity = slots // ep_count
    own_rows = mixing.shape[0]
    hidden_width = expert_weights[0].shape[2]
    shared_width = expert_weights[3].shape[1]
    tokens = ep_count * 2 * half
    model = out_proj.shape[1]
    share = 2 * half // tp_count
    y_count = tp_count // 2
    lam = jnp.broadcast_to(lambdas[:, None, None], (head_count, 8, 128))
    dma = pltpu.SemaphoreType.DMA
    bf16 = jnp.bfloat16
    return pl.pallas_call(
        functools.partial(mixer_kernel, ep_count, tp_count),
        out_shape=(
            jax.ShapeDtypeStruct((share, model), bf16),
            jax.ShapeDtypeStruct((own_rows, model), bf16),
        ),
        in_specs=[pl.BlockSpec(memory_space=pltpu.VMEM)] * 7
        + [pl.BlockSpec(memory_space=pl.ANY)] * 10,
        out_specs=[pl.BlockSpec(memory_space=pltpu.VMEM)] * 2,
        scratch_shapes=[
            pltpu.VMEM((3,) + sequence[0].shape, bf16),
            pltpu.VMEM((3, head_count, 2, half, width), bf16),
            dma((3,)),
            pltpu.VMEM(out_proj.shape, bf16),
            pltpu.VMEM((model, hidden_width), bf16),
            pltpu.VMEM((model, hidden_width), bf16),
            pltpu.VMEM((hidden_width, model), bf16),
            pltpu.VMEM((model, shared_width), bf16),
            pltpu.VMEM((model, shared_width), bf16),
            pltpu.VMEM((shared_width, model), bf16),
            pltpu.VMEM((tp_count, ep_count, capacity, model), bf16),
            pltpu.VMEM((tp_count, slots, hidden_width), bf16),
            pltpu.VMEM((y_count, own_rows + slots, model), bf16),
            pltpu.VMEM((y_count, own_rows + slots, model), bf16),
            pltpu.VMEM((y_count, own_rows + slots, model), bf16),
            pltpu.VMEM((max(1, y_count - 1), own_rows + slots, model), bf16),
            pltpu.VMEM((own_rows, model), jnp.float32),
            pltpu.VMEM((ep_count, capacity, model), bf16),
            pltpu.VMEM((ep_count, capacity, model), bf16),
            dma((7,)),
            dma((ep_count,)),
            dma((ep_count,)),
            dma((ep_count, y_count)),
            dma((ep_count, y_count)),
            dma((ep_count, max(1, y_count - 1))),
            dma((ep_count, max(1, y_count - 1))),
            dma((2,)),
            dma((max(1, y_count - 1),)),
            dma((max(1, y_count - 1),)),
            dma((ep_count,)),
            dma((ep_count,)),
            pltpu.VMEM((tokens // 2, width), bf16),
            pltpu.VMEM((tokens, width), bf16),
            pltpu.VMEM((tokens, width), bf16),
            pltpu.VMEM((head_count, 8, 128), jnp.float32),
            pltpu.VMEM((ep_count, half, width), bf16),
            pltpu.VMEM((head_count, 2 * half, width), bf16),
            pltpu.VMEM((y_count * share, model), bf16),
            pltpu.VMEM((y_count * share, model), bf16),
            pltpu.VMEM((y_count, share, model), bf16),
            pltpu.VMEM((max(1, y_count - 1), share, model), bf16),
            dma((3, head_count, 2)),
            dma((3, ep_count)),
            dma((3,)),
            dma((2, ep_count)),
            dma((2, ep_count)),
            dma((2,)),
            dma((ep_count,)),
            dma((head_count, 2)),
            dma((1,)),
            dma((1,)),
            dma((max(1, y_count - 1),)),
            dma((max(1, y_count - 1),)),
        ],
        compiler_params=pltpu.CompilerParams(
            has_side_effects=True, vmem_limit_bytes=48 * 1024 * 1024
        ),
        name="mixer",
    )(*tables, lam, head_gain[None, :], *prepared, *sequence, out_proj, *expert_weights)


def local(
    queries,
    key_rows,
    value_rows,
    lambdas,
    head_gain,
    out_proj,
    moe_input,
    moe_gain,
    routes,
    route_weights,
    expert_gate,
    expert_up,
    expert_down,
    shared_gate,
    shared_up,
    shared_down,
):
    query_rows = queries.shape[0]
    head_count = lambdas.shape[0]
    head_dim = queries.shape[1] // (2 * head_count)
    tp_count = lax.axis_size("tp")
    ep_count = lax.axis_size("ep")
    tp_place = lax.axis_index("tp")
    ep_place = lax.axis_index("ep")
    positions = ep_place * query_rows + jnp.arange(query_rows, dtype=jnp.int32)
    batch_rows = moe_input.shape[0]
    top_count = routes.shape[1]
    own_rows = batch_rows // tp_count
    local_experts = expert_gate.shape[0]
    expert_count = local_experts * ep_count
    capacity = (2 * own_rows * top_count + expert_count - 1) // expert_count
    one_head_each = ep_count == 2 * head_count and tp_count % 2 == 0 and local_experts == 1
    if one_head_each:
        prepared = prepare(
            moe_input, moe_gain, routes, route_weights, tp_count, expert_count, capacity
        )
        tables = rotation_tables(positions, head_dim)
        sequence = (queries, key_rows, value_rows)
        weights = (expert_gate, expert_up, expert_down, shared_gate, shared_up, shared_down)
        return mixer(
            tables, sequence, lambdas, head_gain, out_proj, prepared, weights, ep_count, tp_count
        )
    else:
        rot_query = rotate(queries, positions, head_dim)
        rot_keys = rotate(key_rows, positions, head_dim)
        initial = (
            jnp.full((head_count, 2, query_rows), -1e30, jnp.float32),
            jnp.zeros((head_count, 2, query_rows), jnp.float32),
            jnp.zeros((head_count, 2, query_rows, 2 * head_dim), jnp.float32),
        )
        running_max, denominator, numerator = fold_keys(
            initial,
            (
                lax.all_gather(rot_keys, "ep", axis=0, tiled=True),
                lax.all_gather(value_rows, "ep", axis=0, tiled=True),
            ),
            rot_query,
            head_count,
            head_dim,
        )
        ratio = numerator / denominator[..., None]
        mixed_heads = ratio[:, 0] - lambdas[:, None, None] * ratio[:, 1]
        mean_square = jnp.mean(mixed_heads * mixed_heads, axis=-1, keepdims=True)
        normed_heads = (mixed_heads * lax.rsqrt(mean_square + head_eps) * head_gain).astype(
            jnp.bfloat16
        )
        head_out = jnp.transpose(normed_heads, (1, 0, 2)).reshape(query_rows, head_count * 2 * head_dim)
    normed = rms_rows(moe_input, moe_gain)
    shared_hidden = gated_hidden(normed, shared_gate, shared_up)
    own_routes = lax.dynamic_slice_in_dim(routes, tp_place * own_rows, own_rows, 0)
    own_weights = lax.dynamic_slice_in_dim(route_weights, tp_place * own_rows, own_rows, 0)
    own_source, own_filled, own_rank = slot_table(own_routes, expert_count, capacity)
    own_normed = lax.dynamic_slice_in_dim(normed, tp_place * own_rows, own_rows, 0)
    outgoing = fill_slots(own_normed, own_source, own_filled)
    arrived = lax.all_to_all(outgoing[:, None], "ep", split_axis=0, concat_axis=2, tiled=True)
    hidden = slot_hidden(lax.all_gather(arrived, "tp", axis=1, tiled=True), expert_gate, expert_up)
    slot_rows = local_experts * ep_count * capacity
    mixer_share = query_rows // tp_count
    expert_share = own_rows + slot_rows
    if not one_head_each:
        block_count = lax.axis_size("tp") * mixer_share // mixer_share
        product = jnp.dot(head_out, out_proj, preferred_element_type=jnp.float32)
        mixer_out = lax.psum_scatter(
            product.reshape(block_count, mixer_share, -1)
            .reshape(lax.axis_size("tp") * mixer_share, -1)
            .astype(jnp.bfloat16),
            "tp",
            scatter_dimension=0,
            tiled=True,
        )
    block_count = lax.axis_size("tp") * expert_share // expert_share
    shared_part = jnp.dot(shared_hidden, shared_down, preferred_element_type=jnp.float32).reshape(
        block_count, own_rows, -1
    )
    routed_part = jnp.einsum(
        "xnsf,xfd->nxsd", hidden, expert_down, preferred_element_type=jnp.float32
    )
    routed_part = routed_part.reshape(block_count, slot_rows, -1)
    expert_sum = lax.psum_scatter(
        jnp.concatenate([shared_part, routed_part], axis=1)
        .reshape(lax.axis_size("tp") * expert_share, -1)
        .astype(jnp.bfloat16),
        "tp",
        scatter_dimension=0,
        tiled=True,
    ).astype(jnp.float32)
    shared_sum = expert_sum[:own_rows]
    routed = (
        expert_sum[own_rows:].reshape(local_experts, ep_count * capacity, -1).astype(jnp.bfloat16)
    )
    returned = lax.all_to_all(routed, "ep", split_axis=1, concat_axis=0, tiled=True)
    flat_index = (own_routes * capacity + own_rank).reshape(-1)
    picked = jnp.take(returned.reshape(expert_count * capacity, -1), flat_index, axis=0).reshape(
        own_rows, top_count, -1
    )
    combined = shared_sum + jnp.sum(own_weights[..., None] * picked.astype(jnp.float32), axis=1)
    return (mixer_out, combined.astype(jnp.bfloat16))


def solution(mesh):
    in_specs = (
        P("ep", "tp"),
        P("ep", "tp"),
        P("ep", "tp"),
        P("tp"),
        P(),
        P("tp", None),
        P("ep", None),
        P(),
        P("ep", None),
        P("ep", None),
        P("ep", None, "tp"),
        P("ep", None, "tp"),
        P("ep", "tp", None),
        P(None, "tp"),
        P(None, "tp"),
        P("tp", None),
    )
    out_specs = (P(("ep", "tp"), None), P(("ep", "tp"), None))
    return jax.shard_map(local, mesh=mesh, in_specs=in_specs, out_specs=out_specs, check_vma=False)
```

profile of v0, /device:TPU:0, one launch (start us, length us, event | category | flops | bytes accessed | tf_op | source)
XLA Modules:
  0.0 110.9 jit_solution(15534046631143700134)
XLA Ops:
  0.7 0.7 broadcast_in_dim.6.lam_ref
  1.4 1.4 %copy.18.routes_ref = s32[128,2]{1,0:T(8,128)} copy(s32[128,2]{0,1:T(2,128)} %param.24) | data formatting | bytes 2048 | tf_op args[8]
  2.8 1.4 %copy.19.scale_ref = f32[128,2]{1,0:T(8,128)} copy(f32[128,2]{0,1:T(2,128)} %param.25) | data formatting | bytes 2048 | tf_op args[9]
  4.2 0.5 fusion
  4.8 0.1 pad_maximum_fusion
  4.9 2.4 %prepare.1 = (bf16[128,2048]{1,0:T(8,128)(2,1)}, bf16[128,2048]{1,0:T(8,128)(2,1)}, f32[32,128]{1,0:T(8,128)}) custom-call(bf16[128,2048]{1,0:T(8,128)(2,1)} %rows_ref.1, f32[1,2048]{1,0:T(1,128)} %bitcast.3, s32[128,2]{1,0:T(8,128)} %copy.18.routes_ref, f32[128,2]{1,0:T(8,128)} %copy.19.scale_ref), custom_call_target="tpu_custom_call" | custom-call | tf_op jit(solution)/shard_map/prepare/pallas_call | solution.py:165
  7.3 0.0 copy-start
  7.3 1.2 %copy-done = bf16[1,2048,256]{2,1,0:T(8,128)(2,1)S(1)} copy-done((bf16[1,2048,256]{2,1,0:T(8,128)(2,1)S(1)}, bf16[1,2048,256]{2,1,0:T(8,128)(2,1)}, u32[]{:S(2)}) %copy-start) | copy-done | bytes 1048600
  8.5 0.0 copy-start.1
  8.5 1.2 %copy-done.1 = bf16[1,2048,256]{2,1,0:T(8,128)(2,1)S(1)} copy-done((bf16[1,2048,256]{2,1,0:T(8,128)(2,1)S(1)}, bf16[1,2048,256]{2,1,0:T(8,128)(2,1)}, u32[]{:S(2)}) %copy-start.1) | copy-done | bytes 1048600
  9.7 0.0 copy-start.2
  9.7 1.0 copy-done.2
  10.8 0.0 copy-start.3
  10.8 1.0 copy-done.3
  11.8 0.0 copy-start.4
  11.8 1.0 copy-done.4
  12.9 0.0 copy-start.5
  12.9 1.0 copy-done.5
  13.9 0.0 copy-start.6
  13.9 1.0 copy-done.6
  15.0 0.0 copy-start.7
  15.0 0.7 copy-done.7
  15.7 0.0 copy-start.8
  15.7 0.7 copy-done.8
  16.4 93.2 %mixer.1 = (bf16[64,2048]{1,0:T(8,128)(2,1)S(1)}, bf16[32,2048]{1,0:T(8,128)(2,1)S(1)}) custom-call(f32[256,128]{1,0:T(8,128)S(1)} %get-tuple-element.11.cos_ref, f32[256,128]{1,0:T(8,128)S(1)} %get-tuple-element.12.sin_ref, f32[4,8,128]{2,1,0:T(8,128)S(1)} %broadcast_in_dim.6.lam_ref, f32[1,256]{1,0:T(1,128)S(1)} %bitcast.2, ...), custom_call_target="tpu_custom_call" | custom-call | tf_op jit(solution)/shard_map/mixer/pallas_call | solution.py:766
  109.6 0.7 copy.22
  110.3 0.7 copy.23
  (2 shorter events, 0.0 us)
Async XLA Ops:
  7.3 1.2 %copy-start = (bf16[1,2048,256]{2,1,0:T(8,128)(2,1)S(1)}, bf16[1,2048,256]{2,1,0:T(8,128)(2,1)}, u32[]{:S(2)}) copy-start(bf16[1,2048,256]{2,1,0:T(8,128)(2,1)} %gate_hbm.1) | copy-start | bytes 3145732
  8.5 1.2 %copy-start.1 = (bf16[1,2048,256]{2,1,0:T(8,128)(2,1)S(1)}, bf16[1,2048,256]{2,1,0:T(8,128)(2,1)}, u32[]{:S(2)}) copy-start(bf16[1,2048,256]{2,1,0:T(8,128)(2,1)} %up_hbm.1) | copy-start | bytes 3145732
  9.7 1.0 copy-start.2
  10.8 1.0 copy-start.3
  11.8 1.0 copy-start.4
  12.9 1.0 copy-start.5
  13.9 1.0 copy-start.6
  15.0 0.7 copy-start.7
  15.7 0.7 copy-start.8
where the time goes:
time: 112 us; the launch traced here: 111 us
  Pallas kernels  95.6 us (85%)
  local copies, waits for them, and re-layouts  14 us (12%)
    pallas_call x1, Pallas kernels, mixer(): pl.pallas_call(functools.partial(mixer_kernel, ep_count, tp_count), out_s...  93.2 us
    unnamed x22, local copies, waits for them, and re-layouts  13.2 us
    pallas_call x1, Pallas kernels, prepare(): pl.pallas_call(functools.partial(prepare_kernel, expert_count, capacity),...  2.4 us

commit v1 on v0

--- a/solution.py
+++ b/solution.py
@@ -128,61 +128,17 @@
     )
 
 
-def prepare_kernel(
-    expert_count, capacity, rows_ref, gain_ref, routes_ref, scale_ref, norm_ref, out_ref, mix_ref
-):
-    own_rows = mix_ref.shape[0]
-    slots = expert_count * capacity
-    widened = rows_ref[...].astype(jnp.float32)
-    mean_square = jnp.mean(widened * widened, axis=-1, keepdims=True)
-    norm_ref[...] = (widened * lax.rsqrt(mean_square + norm_eps) * gain_ref[...]).astype(
-        jnp.bfloat16
-    )
-    own = pl.ds(pl.multiple_of(lax.axis_index("tp") * own_rows, own_rows), own_rows)
-    routes = routes_ref[own, :]
-    scales = scale_ref[own, :]
-    lane = lax.broadcasted_iota(jnp.int32, (own_rows, slots), 1)
-    lane_expert, lane_slot = lane // capacity, lax.rem(lane, capacity)
-    hits = [routes[:, k : k + 1] == lane_expert for k in range(routes.shape[1])]
-    named = sum(hit.astype(jnp.float32) for hit in hits).astype(jnp.bfloat16)
-    row_at = lax.broadcasted_iota(jnp.int32, (own_rows, own_rows), 0)
-    other_at = lax.broadcasted_iota(jnp.int32, (own_rows, own_rows), 1)
-    earlier = (other_at < row_at).astype(jnp.float32).astype(jnp.bfloat16)
-    before = jnp.dot(earlier, named, preferred_element_type=jnp.float32).astype(jnp.int32)
-    chosen = [jnp.logical_and(hit, before == lane_slot).astype(jnp.float32) for hit in hits]
-    mix_ref[...] = sum(scales[:, k : k + 1] * chosen[k] for k in range(len(chosen)))
-    out_ref[...] = lax.dot_general(
-        sum(chosen).astype(jnp.bfloat16),
-        norm_ref[own, :],
-        (((0,), (0,)), ((), ())),
-        preferred_element_type=jnp.float32,
-    ).astype(jnp.bfloat16)
-
-
-def prepare(moe_input, moe_gain, routes, route_weights, tp_count, expert_count, capacity):
-    rows, model = moe_input.shape
-    slots = expert_count * capacity
-    return pl.pallas_call(
-        functools.partial(prepare_kernel, expert_count, capacity),
-        out_shape=(
-            jax.ShapeDtypeStruct((rows, model), jnp.bfloat16),
-            jax.ShapeDtypeStruct((slots, model), jnp.bfloat16),
-            jax.ShapeDtypeStruct((rows // tp_count, slots), jnp.float32),
-        ),
-        name="prepare",
-    )(moe_input, moe_gain[None, :], routes, route_weights)
-
-
 def mixer_kernel(
     ep_count,
     tp_count,
     cos_ref,
     sin_ref,
     lam_ref,
-    gain_ref,
-    norm_ref,
-    slot_ref,
-    mix_ref,
+    gain_hbm,
+    mgain_hbm,
+    routes_hbm,
+    scale_hbm,
+    rows_hbm,
     q_hbm,
     k_hbm,
     v_hbm,
@@ -195,6 +151,15 @@
     sdown_hbm,
     out_ref,
     moe_ref,
+    gain_ref,
+    mgain_ref,
+    routes_ref,
+    scale_ref,
+    rows_ref,
+    small_sem,
+    norm_ref,
+    slot_ref,
+    mix_ref,
     raw,
     pack_ref,
     q_sem,
@@ -229,11 +194,13 @@
     qbuf,
     kbuf,
     vbuf,
+    lam_own,
     lam_other,
     obuf,
     heads,
     sum_out,
     sum_in,
+    kept,
     block_out,
     block_in,
     s_send,
@@ -258,6 +225,23 @@
     partner = y * 2 + 1 - c
     s_me, h_me = e // head_count, lax.rem(e, head_count)
     y_count = tp_count // 2
+    share = half // y_count
+
+    barrier = pltpu.get_barrier_semaphore()
+
+    def greet(where):
+        pl.semaphore_signal(barrier, inc=1, device_id=where, device_id_type=MESH)
+
+    def greet_row(j, carry):
+        there = lax.rem(e + j, ep_count)
+        for core in range(2):
+            greet((there, y * 2 + core))
+        return carry
+
+    lax.fori_loop(1, ep_count, greet_row, 0)
+    greet((e, partner))
+    for step in range(1, y_count):
+        greet((e, lax.rem(y + step, y_count) * 2 + c))
 
     def remote(src, dst, send, recv, where):
         return pltpu.make_async_remote_copy(
@@ -269,31 +253,20 @@
             device_id_type=MESH,
         )
 
-    def landing(which, side, source):
-        if which == 0:
-            return qbuf.at[pl.ds(source * half, half)]
-        return (kbuf, vbuf)[which - 1].at[pl.ds((side * ep_count + source) * half, half)]
-
-    def first_copy(which, h, side):
-        return remote(
-            pack_ref.at[which, h, side],
-            landing(which, side, e),
-            s_send.at[which, h, side],
-            s_recv.at[which, e],
-            (c * head_count + h, y * 2 + side),
-        )
-
-    def own_copy(which):
-        return pltpu.make_async_copy(
-            pack_ref.at[which, h_me, c], landing(which, c, e), s_local.at[which]
-        )
-
-    def forward(which, source):
-        place = landing(which, c, source)
-        return remote(
-            place, place, f_send.at[which - 1, source], f_recv.at[which - 1, source], (e, partner)
-        )
-
+    small_copies = [
+        pltpu.make_async_copy(a, b, small_sem.at[at])
+        for at, (a, b) in enumerate(
+            (
+                (rows_hbm, rows_ref),
+                (mgain_hbm, mgain_ref),
+                (routes_hbm, routes_ref),
+                (scale_hbm, scale_ref),
+                (gain_hbm, gain_ref),
+            )
+        )
+    ]
+    for copy in small_copies:
+        copy.start()
     raw_copies = [
         pltpu.make_async_copy(ref, raw.at[at], q_sem.at[at])
         for at, ref in enumerate((q_hbm, k_hbm, v_hbm))
@@ -317,57 +290,67 @@
     for copy in weight_copies:
         copy.start()
 
+    def landing(which, side, source):
+        if which == 0:
+            return qbuf.at[source]
+        return (kbuf, vbuf)[which - 1].at[pl.ds((side * ep_count + source) * half, half)]
+
+    def first_copy(which, h, side):
+        return remote(
+            pack_ref.at[which, h, side],
+            landing(which, side, e),
+            s_send.at[which, h, side],
+            s_recv.at[which, e],
+            (c * head_count + h, y * 2 + side),
+        )
+
+    def own_copy(which):
+        return pltpu.make_async_copy(
+            pack_ref.at[which, h_me, c], landing(which, c, e), s_local.at[which]
+        )
+
+    def forward(which, source):
+        place = landing(which, c, source)
+        return remote(
+            place, place, f_send.at[which - 1, source], f_recv.at[which - 1, source], (e, partner)
+        )
+
     capacity = xbuf.shape[2]
     own_rows = moe_ref.shape[0]
     slots = ep_count * capacity
-
-    def dispatch(target):
-        rows = pl.ds(pl.multiple_of(target * capacity, capacity), capacity)
-        return remote(
-            slot_ref.at[rows], xbuf.at[t, e], d_send.at[target], d_recv.at[e], (target, t)
-        )
-
-    own_slots = pl.ds(pl.multiple_of(e * capacity, capacity), capacity)
-    own_dispatch = pltpu.make_async_copy(slot_ref.at[own_slots], xbuf.at[t, e], d_recv.at[e])
-    own_dispatch.start()
-
-    def start_dispatch(j, carry):
-        dispatch(lax.rem(e + 1 + j, ep_count)).start()
-        return carry
-
-    lax.fori_loop(0, ep_count - 1, start_dispatch, 0)
-
-    lam_copy = remote(lam_ref, lam_other, l_sem.at[0], l_sem.at[1], (e, partner))
-    lam_copy.start()
-
-    mine = s_me == c
-
-    def each_send(act):
-        def body(j, carry):
-            h = lax.rem(h_me + 1 + j, head_count)
-            for k in range(2):
-                side = lax.rem(c + 1 + k, 2)
-                own = jnp.logical_and(c * head_count + h == e, side == c)
-                act(h, side, own)
-            return carry
-
-        lax.fori_loop(0, head_count, body, 0)
-
-    def start_send(h, side, own):
-        @pl.when(jnp.logical_not(own))
-        def _():
-            for which in range(3):
-                first_copy(which, h, side).start()
-
-        @pl.when(own)
-        def _():
-            for which in range(3):
-                own_copy(which).start()
+    batch_rows = rows_ref.shape[0]
+
+    for copy in small_copies[:4]:
+        copy.wait()
+    widened = rows_ref[...].astype(jnp.float32)
+    mean_square = jnp.mean(widened * widened, axis=-1, keepdims=True)
+    norm_ref[...] = (widened * lax.rsqrt(mean_square + norm_eps) * mgain_ref[...]).astype(
+        jnp.bfloat16
+    )
+    slot_at = lax.broadcasted_iota(jnp.int32, (slots, batch_rows), 0)
+    slot_expert, slot_rank = slot_at // capacity, lax.rem(slot_at, capacity)
+    hits = [routes_ref[k : k + 1, :] == slot_expert for k in range(routes_ref.shape[0])]
+    named = sum(hit.astype(jnp.float32) for hit in hits).astype(jnp.bfloat16)
+    other_at = lax.broadcasted_iota(jnp.int32, (batch_rows, batch_rows), 0)
+    row_at = lax.broadcasted_iota(jnp.int32, (batch_rows, batch_rows), 1)
+    earlier = jnp.logical_and(other_at < row_at, other_at // own_rows == row_at // own_rows)
+    before = jnp.dot(
+        named, earlier.astype(jnp.float32).astype(jnp.bfloat16), preferred_element_type=jnp.float32
+    ).astype(jnp.int32)
+    chosen = [jnp.logical_and(hit, before == slot_rank).astype(jnp.float32) for hit in hits]
+    token_block = lax.broadcasted_iota(jnp.int32, (slots, batch_rows), 1) // own_rows
+    picked = jnp.where(token_block == t, sum(chosen), 0.0).astype(jnp.bfloat16)
+    slot_ref[...] = jnp.dot(
+        picked, norm_ref[...], preferred_element_type=jnp.float32
+    ).astype(jnp.bfloat16)
+    mixing = sum(scale_ref[k : k + 1, :] * chosen[k] for k in range(len(chosen)))
+    mix_ref[...] = jnp.transpose(mixing)
+    lam_own[...] = jnp.full(lam_own.shape, lam_ref[h_me], jnp.float32)
 
     for copy in raw_copies:
         copy.wait()
 
-    def pack_head(h):
+    def pack_head(h, carry):
         cosine = cos_ref[...]
         sines = sin_ref[...]
         for which in range(2):
@@ -376,31 +359,79 @@
                 part = raw[which, :, pl.ds(at, head_dim)].astype(jnp.float32)
                 turned = part * cosine + pltpu.roll(part, head_dim // 2, 1) * sines
                 turned = turned.astype(jnp.bfloat16)
-                for side in range(2):
-                    pack_ref[which, h, side, :, m * head_dim : (m + 1) * head_dim] = turned[
-                        side * half : (side + 1) * half
-                    ]
+                for v in range(y_count):
+                    for side in range(2):
+                        block = v * 2 + side
+                        pack_ref[
+                            which,
+                            h,
+                            side,
+                            v * share : (v + 1) * share,
+                            m * head_dim : (m + 1) * head_dim,
+                        ] = turned[block * share : (block + 1) * share]
         at = pl.multiple_of(h * width, width)
-        for side in range(2):
-            pack_ref[2, h, side] = raw[2, side * half : (side + 1) * half, pl.ds(at, width)]
-
-    def head_at(j):
-        return lax.rem(h_me + 1 + j, head_count)
-
-    def send_head(h):
-        for k in range(2):
-            side = lax.rem(c + 1 + k, 2)
-            start_send(h, side, jnp.logical_and(c * head_count + h == e, side == c))
-
-    pack_head(head_at(0))
-
-    def pack_and_send(j, carry):
-        pack_head(head_at(j))
-        send_head(head_at(j - 1))
-        return carry
-
-    lax.fori_loop(1, head_count, pack_and_send, 0)
-    send_head(head_at(head_count - 1))
+        for v in range(y_count):
+            for side in range(2):
+                block = v * 2 + side
+                pack_ref[2, h, side, v * share : (v + 1) * share] = raw[
+                    2, block * share : (block + 1) * share, pl.ds(at, width)
+                ]
+        return carry
+
+    lax.fori_loop(0, head_count, pack_head, 0)
+
+    pl.semaphore_wait(barrier, (ep_count - 1) * 2 + 1 + (y_count - 1))
+
+    def dispatch(target):
+        rows = pl.ds(pl.multiple_of(target * capacity, capacity), capacity)
+        return remote(
+            slot_ref.at[rows], xbuf.at[t, e], d_send.at[target], d_recv.at[e], (target, t)
+        )
+
+    own_slots = pl.ds(pl.multiple_of(e * capacity, capacity), capacity)
+    own_dispatch = pltpu.make_async_copy(slot_ref.at[own_slots], xbuf.at[t, e], d_recv.at[e])
+
+    def start_dispatch(j, carry):
+        dispatch(lax.rem(e + ep_count // 2 + j, ep_count)).start()
+        return carry
+
+    lax.fori_loop(0, ep_count // 2, start_dispatch, 0)
+
+    def start_late(j, carry):
+        dispatch(lax.rem(e + 1 + j, ep_count)).start()
+        return carry
+
+    lax.fori_loop(0, ep_count // 2 - 1, start_late, 0)
+
+    mine = s_me == c
+
+    def each_send(whiches, act):
+        def body(j, carry):
+            h = lax.rem(h_me + 1 + j, head_count)
+            for k in range(2):
+                side = lax.rem(c + 1 + k, 2)
+                own = jnp.logical_and(c * head_count + h == e, side == c)
+                act(whiches, h, side, own)
+            return carry
+
+        lax.fori_loop(0, head_count, body, 0)
+
+    def start_send(whiches, h, side, own):
+        @pl.when(jnp.logical_not(own))
+        def _():
+            for which in whiches:
+                first_copy(which, h, side).start()
+
+    each_send((1, 2), start_send)
+    each_send((0,), start_send)
+    lam_copy = remote(lam_own, lam_other, l_sem.at[0], l_sem.at[1], (e, partner))
+    lam_copy.start()
+    own_dispatch.start()
+
+    @pl.when(mine)
+    def _():
+        for which in range(3):
+            own_copy(which).start()
 
     for copy in weight_copies[:3]:
         copy.wait()
@@ -516,27 +547,36 @@
 
     for step in range(1, y_count):
         far_copy(step).start()
+
+    def arrived(which, source):
+        own = jnp.logical_and(source == e, mine)
+
+        @pl.when(own)
+        def _():
+            own_copy(which).wait()
+
+        @pl.when(jnp.logical_not(own))
+        def _():
+            place = landing(which, c, source)
+            remote(
+                place, place, f_send.at[0, source], s_recv.at[which, source], (e, partner)
+            ).wait_recv()
+
     def arrive(j, carry):
         source = lax.rem(e + j, ep_count)
-        own = jnp.logical_and(source == e, mine)
-        for which in range(3):
-
-            @pl.when(own)
-            def _():
-                own_copy(which).wait()
-
-            @pl.when(jnp.logical_not(own))
-            def _():
-                place = landing(which, c, source)
-                remote(
-                    place, place, f_send.at[0, source], s_recv.at[which, source], (e, partner)
-                ).wait_recv()
-
-            if which > 0:
-                forward(which, source).start()
+        for which in (1, 2):
+            arrived(which, source)
+            forward(which, source).start()
         return carry
 
     lax.fori_loop(0, ep_count, arrive, 0)
+
+    def give_back(target):
+        return remote(
+            ret_out.at[target], ret_in.at[e], v_send.at[target], v_recv.at[e], (target, t)
+        )
+
+    own_back = pltpu.make_async_copy(ret_out.at[e], ret_in.at[e], v_recv.at[e])
 
     for step in range(1, y_count):
         far_copy(step).wait_recv()
@@ -546,19 +586,12 @@
     shared_sum[...] = expert_sum[:own_rows]
     ret_out[...] = expert_sum[own_rows:].astype(jnp.bfloat16).reshape(ret_out.shape)
 
-    def give_back(target):
-        return remote(
-            ret_out.at[target], ret_in.at[e], v_send.at[target], v_recv.at[e], (target, t)
-        )
-
-    own_back = pltpu.make_async_copy(ret_out.at[e], ret_in.at[e], v_recv.at[e])
-    own_back.start()
-
     def start_back(j, carry):
         give_back(lax.rem(e + 1 + j, ep_count)).start()
         return carry
 
     lax.fori_loop(0, ep_count - 1, start_back, 0)
+    own_back.start()
 
     def arrive_forward(j, carry):
         source = lax.rem(e + j, ep_count)
@@ -575,28 +608,42 @@
 
     lax.fori_loop(0, ep_count, arrive_forward, 0)
     lam_copy.wait()
-
-    lam = jnp.where(mine, lam_ref[h_me], lam_other[h_me])[0:1, 0:1]
+    small_copies[4].wait()
+
+    lam = jnp.where(mine, lam_own[...], lam_other[...])[0:1, 0:1]
     gain = gain_ref[...]
     factor = head_dim ** (-0.5) * log2_e
 
-    def back_copy(target):
+    def back_place(v):
+        return heads.at[h_me, v, c]
+
+    def back_copy(target, v):
         return remote(
-            obuf.at[target],
-            heads.at[h_me, pl.ds(c * half, half)],
-            o_send.at[target],
-            o_recv.at[h_me, c],
+            obuf.at[target, v],
+            back_place(v),
+            o_send.at[target, v],
+            o_recv.at[h_me, v, c],
             (target, y * 2 + s_me),
         )
 
-    def back_own():
-        return pltpu.make_async_copy(
-            obuf.at[e], heads.at[h_me, pl.ds(c * half, half)], o_recv.at[h_me, c]
-        )
+    def back_own(v):
+        return pltpu.make_async_copy(obuf.at[e, v], back_place(v), o_recv.at[h_me, v, c])
+
+    pair_count = ep_count // 2
+    pair_me = e // 2
 
     def attend(j, carry):
-        target = lax.rem(e + 1 + j, ep_count)
-        block = qbuf[pl.ds(target * half, half), :]
+        v = lax.rem(y + 1 + j // pair_count, y_count)
+        at = lax.rem(pair_me + pair_count // 2 + lax.rem(j, pair_count), pair_count)
+        targets = (at * 2, at * 2 + 1)
+
+        @pl.when(j < pair_count)
+        def _():
+            for target in targets:
+                arrived(0, target)
+
+        rows = pl.ds(pl.multiple_of(v * share, share), share)
+        block = jnp.concatenate([qbuf[target, rows, :] for target in targets], axis=0)
         ratios = []
         for m in range(2):
             columns = slice(m * head_dim, (m + 1) * head_dim)
@@ -615,20 +662,84 @@
             ratios.append(weighted / denominator)
         mixed = ratios[0] - lam * ratios[1]
         mean_square = jnp.mean(mixed * mixed, axis=-1, keepdims=True)
-        obuf[target] = (mixed * lax.rsqrt(mean_square + head_eps) * gain).astype(jnp.bfloat16)
-        own = jnp.logical_and(target == e, mine)
-
-        @pl.when(jnp.logical_not(own))
-        def _():
-            back_copy(target).start()
-
-        @pl.when(own)
-        def _():
-            back_own().start()
-
-        return carry
-
-    lax.fori_loop(0, ep_count, attend, 0)
+        done = (mixed * lax.rsqrt(mean_square + head_eps) * gain).astype(jnp.bfloat16)
+        for k, target in enumerate(targets):
+            obuf[target, v] = done[k * share : (k + 1) * share]
+        for target in targets:
+            own = jnp.logical_and(target == e, mine)
+
+            @pl.when(jnp.logical_not(own))
+            def _():
+                back_copy(target, v).start()
+
+            @pl.when(own)
+            def _():
+                back_own(v).start()
+
+        return carry
+
+    lax.fori_loop(0, pair_count * y_count, attend, 0)
+
+    weight_copies[6].wait()
+
+    def pair_copy(at):
+        return remote(sum_out.at[at], sum_in.at[at], r_send.at[at], r_recv.at[at], (e, partner))
+
+    def project(at):
+        v = lax.rem(y + 1 + at, y_count)
+
+        def arrive_heads(h, carry):
+            for side in range(2):
+                own = jnp.logical_and(
+                    jnp.logical_and(c * head_count + h == e, side == c), h == h_me
+                )
+                place = heads.at[h, v, side]
+
+                @pl.when(own)
+                def _():
+                    back_own(v).wait()
+
+                @pl.when(jnp.logical_not(own))
+                def _():
+                    remote(
+                        place, place, o_send.at[0, 0], o_recv.at[h, v, side], (e, partner)
+                    ).wait_recv()
+
+            return carry
+
+        lax.fori_loop(0, head_count, arrive_heads, 0)
+        total = None
+        for h in range(head_count):
+            rows = jnp.concatenate([heads[h, v, 1 - c], heads[h, v, c]], axis=0)
+            term = jnp.dot(
+                rows,
+                proj_ref[h * width : (h + 1) * width, :],
+                preferred_element_type=jnp.float32,
+            )
+            total = term if total is None else total + term
+        total = total.astype(jnp.bfloat16)
+        sum_out[at] = total[:share]
+        kept[at] = total[share:]
+        pair_copy(at).start()
+
+    def block_copy(step):
+        target = lax.rem(y + step, y_count)
+        return remote(
+            block_out.at[step - 1],
+            block_in.at[step - 1],
+            b_send.at[step - 1],
+            b_recv.at[step - 1],
+            (e, target * 2 + c),
+        )
+
+    for step in range(1, y_count):
+        project(step - 1)
+        pair_copy(step - 1).wait()
+        block_out[step - 1] = (
+            kept[step - 1].astype(jnp.float32) + sum_in[step - 1].astype(jnp.float32)
+        ).astype(jnp.bfloat16)
+        block_copy(step).start()
+    project(y_count - 1)
 
     own_back.wait()
 
@@ -639,7 +750,7 @@
         return carry
 
     lax.fori_loop(0, ep_count - 1, arrive_back, 0)
-    mix = mix_ref[...]
+    mix = mix_ref[pl.ds(pl.multiple_of(t * own_rows, own_rows), own_rows), :]
     coarse = mix.astype(jnp.bfloat16)
     fine = (mix - coarse.astype(jnp.float32)).astype(jnp.bfloat16)
     returned = ret_in[...].reshape(slots, ret_in.shape[2])
@@ -647,76 +758,23 @@
     combined = combined + jnp.dot(fine, returned, preferred_element_type=jnp.float32)
     moe_ref[...] = (shared_sum[...] + combined).astype(jnp.bfloat16)
 
-    def arrive_heads(h, carry):
-        for side in range(2):
-            own = jnp.logical_and(c * head_count + h == e, side == c)
-            place = heads.at[h, pl.ds(side * half, half)]
-
-            @pl.when(own)
-            def _():
-                back_own().wait()
-
-            @pl.when(jnp.logical_not(own))
-            def _():
-                remote(
-                    place, place, o_send.at[0], o_recv.at[h, side], (e, partner)
-                ).wait_recv()
-
-        return carry
-
-    lax.fori_loop(0, head_count, arrive_heads, 0)
-
-    weight_copies[6].wait()
-    share = out_ref.shape[0]
-
-    def partial(core):
-        total = None
-        for h in range(head_count):
-            rows = jnp.concatenate(
-                [heads[h, pl.ds((v * 2 + core) * share, share), :] for v in range(y_count)], axis=0
-            )
-            term = jnp.dot(
-                rows,
-                proj_ref[h * width : (h + 1) * width, :],
-                preferred_element_type=jnp.float32,
-            )
-            total = term if total is None else total + term
-        return total.astype(jnp.bfloat16)
-
-    sum_out[...] = partial(1 - c)
-    pair_copy = remote(sum_out, sum_in, r_send.at[0], r_recv.at[0], (e, partner))
-    pair_copy.start()
-    kept = partial(c).astype(jnp.float32)
-    pair_copy.wait()
-    block_out[...] = (
-        (kept + sum_in[...].astype(jnp.float32)).astype(jnp.bfloat16).reshape(block_out.shape)
-    )
-
-    def block_copy(step):
-        target = lax.rem(y + step, y_count)
-        return remote(
-            block_out.at[target],
-            block_in.at[step - 1],
-            b_send.at[step - 1],
-            b_recv.at[step - 1],
-            (e, target * 2 + c),
-        )
-
-    for step in range(1, y_count):
-        block_copy(step).start()
-    total = block_out[y].astype(jnp.float32)
+    pair_copy(y_count - 1).wait()
+    total = (
+        kept[y_count - 1].astype(jnp.float32) + sum_in[y_count - 1].astype(jnp.float32)
+    ).astype(jnp.bfloat16)
+    total = total.astype(jnp.float32)
     for step in range(1, y_count):
         block_copy(step).wait()
         total = total + block_in[step - 1].astype(jnp.float32)
     out_ref[...] = total.astype(jnp.bfloat16)
 
-    def end_send(h, side, own):
+    def end_send(whiches, h, side, own):
         @pl.when(jnp.logical_not(own))
         def _():
-            for which in range(3):
+            for which in whiches:
                 first_copy(which, h, side).wait_send()
 
-    each_send(end_send)
+    each_send((0, 1, 2), end_send)
 
     for step in range(1, y_count):
         far_copy(step).wait_send()
@@ -737,7 +795,8 @@
 
         @pl.when(jnp.logical_not(jnp.logical_and(source == e, mine)))
         def _():
-            back_copy(source).wait_send()
+            for v in range(y_count):
+                back_copy(source, v).wait_send()
 
         return carry
 
@@ -745,22 +804,30 @@
 
 
 def mixer(
-    tables, sequence, lambdas, head_gain, out_proj, prepared, expert_weights, ep_count, tp_count
+    tables,
+    sequence,
+    lambdas,
+    head_gain,
+    out_proj,
+    moe_inputs,
+    expert_weights,
+    ep_count,
+    tp_count,
+    capacity,
 ):
-    normed, outgoing, mixing = prepared
+    moe_input, moe_gain, routes, route_weights = moe_inputs
     head_count = lambdas.shape[0]
     half = sequence[0].shape[0] // 2
     width = sequence[0].shape[1] // head_count
-    slots = outgoing.shape[0]
-    capacity = slots // ep_count
-    own_rows = mixing.shape[0]
+    slots = ep_count * capacity
+    batch_rows, model = moe_input.shape
+    own_rows = batch_rows // tp_count
+    top_count = routes.shape[1]
     hidden_width = expert_weights[0].shape[2]
     shared_width = expert_weights[3].shape[1]
     tokens = ep_count * 2 * half
-    model = out_proj.shape[1]
     share = 2 * half // tp_count
     y_count = tp_count // 2
-    lam = jnp.broadcast_to(lambdas[:, None, None], (head_count, 8, 128))
     dma = pltpu.SemaphoreType.DMA
     bf16 = jnp.bfloat16
     return pl.pallas_call(
@@ -769,10 +836,20 @@
             jax.ShapeDtypeStruct((share, model), bf16),
             jax.ShapeDtypeStruct((own_rows, model), bf16),
         ),
-        in_specs=[pl.BlockSpec(memory_space=pltpu.VMEM)] * 7
-        + [pl.BlockSpec(memory_space=pl.ANY)] * 10,
+        in_specs=[pl.BlockSpec(memory_space=pltpu.VMEM)] * 2
+        + [pl.BlockSpec(memory_space=pltpu.SMEM)]
+        + [pl.BlockSpec(memory_space=pltpu.HBM)] * 15,
         out_specs=[pl.BlockSpec(memory_space=pltpu.VMEM)] * 2,
         scratch_shapes=[
+            pltpu.VMEM((1, width), jnp.float32),
+            pltpu.VMEM((1, model), jnp.float32),
+            pltpu.VMEM((top_count, batch_rows), jnp.int32),
+            pltpu.VMEM((top_count, batch_rows), jnp.float32),
+            pltpu.VMEM((batch_rows, model), bf16),
+            dma((5,)),
+            pltpu.VMEM((batch_rows, model), bf16),
+            pltpu.VMEM((slots, model), bf16),
+            pltpu.VMEM((batch_rows, slots), jnp.float32),
             pltpu.VMEM((3,) + sequence[0].shape, bf16),
             pltpu.VMEM((3, head_count, 2, half, width), bf16),
             dma((3,)),
@@ -804,15 +881,17 @@
             dma((max(1, y_count - 1),)),
             dma((ep_count,)),
             dma((ep_count,)),
-            pltpu.VMEM((tokens // 2, width), bf16),
+            pltpu.VMEM((ep_count, half, width), bf16),
             pltpu.VMEM((tokens, width), bf16),
             pltpu.VMEM((tokens, width), bf16),
-            pltpu.VMEM((head_count, 8, 128), jnp.float32),
-            pltpu.VMEM((ep_count, half, width), bf16),
-            pltpu.VMEM((head_count, 2 * half, width), bf16),
-            pltpu.VMEM((y_count * share, model), bf16),
-            pltpu.VMEM((y_count * share, model), bf16),
+            pltpu.VMEM((8, 128), jnp.float32),
+            pltpu.VMEM((8, 128), jnp.float32),
+            pltpu.VMEM((ep_count, y_count, share, width), bf16),
+            pltpu.VMEM((head_count, y_count, 2, share, width), bf16),
             pltpu.VMEM((y_count, share, model), bf16),
+            pltpu.VMEM((y_count, share, model), bf16),
+            pltpu.VMEM((y_count, share, model), bf16),
+            pltpu.VMEM((max(1, y_count - 1), share, model), bf16),
             pltpu.VMEM((max(1, y_count - 1), share, model), bf16),
             dma((3, head_count, 2)),
             dma((3, ep_count)),
@@ -820,18 +899,29 @@
             dma((2, ep_count)),
             dma((2, ep_count)),
             dma((2,)),
-            dma((ep_count,)),
-            dma((head_count, 2)),
-            dma((1,)),
-            dma((1,)),
+            dma((ep_count, y_count)),
+            dma((head_count, y_count, 2)),
+            dma((y_count,)),
+            dma((y_count,)),
             dma((max(1, y_count - 1),)),
             dma((max(1, y_count - 1),)),
         ],
         compiler_params=pltpu.CompilerParams(
-            has_side_effects=True, vmem_limit_bytes=48 * 1024 * 1024
+            has_side_effects=True, vmem_limit_bytes=67043328, collective_id=0
         ),
         name="mixer",
-    )(*tables, lam, head_gain[None, :], *prepared, *sequence, out_proj, *expert_weights)
+    )(
+        *tables,
+        lambdas,
+        head_gain[None, :],
+        moe_gain[None, :],
+        jnp.transpose(routes),
+        jnp.transpose(route_weights),
+        moe_input,
+        *sequence,
+        out_proj,
+        *expert_weights,
+    )
 
 
 def local(
@@ -866,16 +956,22 @@
     local_experts = expert_gate.shape[0]
     expert_count = local_experts * ep_count
     capacity = (2 * own_rows * top_count + expert_count - 1) // expert_count
-    one_head_each = ep_count == 2 * head_count and tp_count % 2 == 0 and local_experts == 1
+    one_head_each = ep_count == 2 * head_count and tp_count % 2 == 0 and local_experts == 1 and ep_count % 4 == 0
     if one_head_each:
-        prepared = prepare(
-            moe_input, moe_gain, routes, route_weights, tp_count, expert_count, capacity
-        )
         tables = rotation_tables(positions, head_dim)
         sequence = (queries, key_rows, value_rows)
         weights = (expert_gate, expert_up, expert_down, shared_gate, shared_up, shared_down)
         return mixer(
-            tables, sequence, lambdas, head_gain, out_proj, prepared, weights, ep_count, tp_count
+            tables,
+            sequence,
+            lambdas,
+            head_gain,
+            out_proj,
+            (moe_input, moe_gain, routes, route_weights),
+            weights,
+            ep_count,
+            tp_count,
+            capacity,
         )
     else:
         rot_query = rotate(queries, positions, head_dim)

time: 112 us -> 97.8 us (0.87)
  local copies, waits for them, and re-layouts: 14 us -> 3.24 us
  Pallas kernels: 95.6 us -> 92.3 us
    unnamed x22 -> x2, local copies, waits for them, and re-layouts: 13.2 us -> 3.24 us
    pallas_call x1 -> x0, Pallas kernels: 2.4 us -> none  [prepare(): pl.pallas_call(functools.partial(prepare_kernel, expert_count, capacity),...]
where the time goes in v1:
time: 97.8 us; the launch traced here: 97.6 us
  Pallas kernels  92.3 us (94%)
  local copies, waits for them, and re-layouts  3.24 us (3%)
  other arithmetic  1.39 us (1%)
    pallas_call x1, Pallas kernels, mixer(): pl.pallas_call(functools.partial(mixer_kernel, ep_count, tp_count), out_s...  92.3 us
    unnamed x2, local copies, waits for them, and re-layouts  3.24 us

profile of v1, /device:TPU:0, one launch (start us, length us, event | category | flops | bytes accessed | tf_op | source)
XLA Modules:
  0.0 97.6 jit_solution(4237144094000295128)
XLA Ops:
  0.7 0.5 fusion
  1.2 0.8 pad_maximum_fusion
  2.0 92.3 %mixer.1 = (bf16[64,2048]{1,0:T(8,128)(2,1)}, bf16[32,2048]{1,0:T(8,128)(2,1)}) custom-call(f32[256,128]{1,0:T(8,128)} %get-tuple-element.5.cos_ref, f32[256,128]{1,0:T(8,128)} %get-tuple-element.6.sin_ref, f32[4]{0:T(128)} %lam_ref.1, f32[1,256]{1,0:T(1,128)} %bitcast.5, f32[1,2048]{1,0:T(1,128)} %bitcast.4, s32[2,128]{1,0:T(2,128)} %bitcast.6, ...), custom_call_target="tpu_custom_call" | custom-call | tf_op jit(solution)/shard_map/mixer/pallas_call | solution.py:833
  94.4 1.7 %copy.20 = bf16[64,2048]{1,0:T(8,128)(2,1)} copy(bf16[64,2048]{1,0:T(8,128)(2,1)} %get-tuple-element.9) | data formatting | bytes 524288
  96.1 1.6 %copy.21 = bf16[32,2048]{1,0:T(8,128)(2,1)} copy(bf16[32,2048]{1,0:T(8,128)(2,1)} %get-tuple-element.10) | data formatting | bytes 262144
  (2 shorter events, 0.0 us)

commit v2 on v1

--- a/solution.py
+++ b/solution.py
@@ -1,6 +1,7 @@
 import functools
 import jax
 import jax.numpy as jnp
+import numpy as np
 from jax import lax
 from jax.experimental import pallas as pl
 from jax.experimental.pallas import tpu as pltpu
@@ -117,23 +118,28 @@
     return jnp.where(filled[..., None], taken, jnp.zeros_like(taken))
 
 
-def rotation_tables(positions, head_dim):
+def rotation_tables(row_count, block_count, head_dim):
     half_dim = head_dim // 2
-    frequency = jnp.power(theta_base, -jnp.arange(half_dim, dtype=jnp.float32) * 2.0 / head_dim)
-    angles = positions.astype(jnp.float32)[:, None] * frequency[None, :]
-    cosine, sines = jnp.cos(angles), jnp.sin(angles)
+    frequency = np.power(theta_base, -np.arange(half_dim) * 2.0 / head_dim)
+
+    def table(positions):
+        angles = positions[:, None] * frequency[None, :]
+        cosine, sines = np.cos(angles), np.sin(angles)
+        both = (np.concatenate([cosine, cosine], 1), np.concatenate([-sines, sines], 1))
+        return np.stack(both).astype(np.float32)
+
     return (
-        jnp.concatenate([cosine, cosine], axis=1),
-        jnp.concatenate([-sines, sines], axis=1),
+        jnp.asarray(table(np.arange(row_count))),
+        jnp.asarray(table(np.arange(block_count) * row_count)),
     )
 
 
 def mixer_kernel(
     ep_count,
     tp_count,
-    cos_ref,
-    sin_ref,
     lam_ref,
+    turn_hbm,
+    base_hbm,
     gain_hbm,
     mgain_hbm,
     routes_hbm,
@@ -151,6 +157,10 @@
     sdown_hbm,
     out_ref,
     moe_ref,
+    turn_ref,
+    base_ref,
+    cos_ref,
+    sin_ref,
     gain_ref,
     mgain_ref,
     routes_ref,
@@ -160,6 +170,12 @@
     norm_ref,
     slot_ref,
     mix_ref,
+    ext_out,
+    ext_in,
+    rel_slots,
+    gathered,
+    part_out,
+    part_in,
     raw,
     pack_ref,
     q_sem,
@@ -182,6 +198,11 @@
     w_sem,
     d_send,
     d_recv,
+    c_sem,
+    k_send,
+    u_send,
+    u_recv,
+    m_sem,
     g_send,
     g_recv,
     h_send,
@@ -257,10 +278,12 @@
         pltpu.make_async_copy(a, b, small_sem.at[at])
         for at, (a, b) in enumerate(
             (
-                (rows_hbm, rows_ref),
-                (mgain_hbm, mgain_ref),
                 (routes_hbm, routes_ref),
                 (scale_hbm, scale_ref),
+                (mgain_hbm, mgain_ref),
+                (rows_hbm, rows_ref),
+                (base_hbm, base_ref),
+                (turn_hbm, turn_ref),
                 (gain_hbm, gain_ref),
             )
         )
@@ -287,9 +310,6 @@
             )
         )
     ]
-    for copy in weight_copies:
-        copy.start()
-
     def landing(which, side, source):
         if which == 0:
             return qbuf.at[source]
@@ -319,6 +339,15 @@
     own_rows = moe_ref.shape[0]
     slots = ep_count * capacity
     batch_rows = rows_ref.shape[0]
+    model = rows_ref.shape[1]
+    half_count = ep_count // 2
+    half_slots = half_count * capacity
+    across = lax.rem(e + half_count, ep_count)
+    near_first = s_me * half_count
+    place_me = lax.rem(e, half_count)
+
+    def near(j):
+        return near_first + lax.rem(place_me + j, half_count)
 
     for copy in small_copies[:4]:
         copy.wait()
@@ -347,6 +376,21 @@
     mix_ref[...] = jnp.transpose(mixing)
     lam_own[...] = jnp.full(lam_own.shape, lam_ref[h_me], jnp.float32)
 
+    def fold(wide):
+        return jnp.where(s_me == 0, wide[:, half_slots:], wide[:, :half_slots])
+
+    own_span = pl.ds(pl.multiple_of(t * own_rows, own_rows), own_rows)
+    away = fold(mix_ref[own_span, :])
+    away_coarse = away.astype(jnp.bfloat16)
+    away_fine = (away - away_coarse.astype(jnp.float32)).astype(jnp.bfloat16)
+    ext_out[:, :model] = norm_ref[own_span, :]
+    ext_out[:, model:] = jnp.concatenate([away_coarse, away_fine], axis=1)
+
+    for copy in small_copies[4:6]:
+        copy.wait()
+    base_cos, base_sin = base_ref[0, pl.ds(e, 1), :], base_ref[1, pl.ds(e, 1), :]
+    cos_ref[...] = base_cos * turn_ref[0] - base_sin * turn_ref[1]
+    sin_ref[...] = base_sin * turn_ref[0] + base_cos * turn_ref[1]
     for copy in raw_copies:
         copy.wait()
 
@@ -382,26 +426,23 @@
 
     pl.semaphore_wait(barrier, (ep_count - 1) * 2 + 1 + (y_count - 1))
 
+    for copy in weight_copies:
+        copy.start()
+
     def dispatch(target):
         rows = pl.ds(pl.multiple_of(target * capacity, capacity), capacity)
         return remote(
             slot_ref.at[rows], xbuf.at[t, e], d_send.at[target], d_recv.at[e], (target, t)
         )
 
-    own_slots = pl.ds(pl.multiple_of(e * capacity, capacity), capacity)
-    own_dispatch = pltpu.make_async_copy(slot_ref.at[own_slots], xbuf.at[t, e], d_recv.at[e])
+    cross_copy = remote(ext_out, ext_in, c_sem.at[0], c_sem.at[1], (across, t))
+    cross_copy.start()
 
     def start_dispatch(j, carry):
-        dispatch(lax.rem(e + ep_count // 2 + j, ep_count)).start()
-        return carry
-
-    lax.fori_loop(0, ep_count // 2, start_dispatch, 0)
-
-    def start_late(j, carry):
-        dispatch(lax.rem(e + 1 + j, ep_count)).start()
-        return carry
-
-    lax.fori_loop(0, ep_count // 2 - 1, start_late, 0)
+        dispatch(near(j)).start()
+        return carry
+
+    lax.fori_loop(1, half_count, start_dispatch, 0)
 
     mine = s_me == c
 
@@ -422,16 +463,20 @@
             for which in whiches:
                 first_copy(which, h, side).start()
 
-    each_send((1, 2), start_send)
-    each_send((0,), start_send)
+    pair_count = ep_count // 2
+    pair_me = e // 2
+    near_pairs = pair_count // 2
+    beside = jnp.logical_or(pair_me == near_pairs - 1, pair_me == near_pairs)
+    at_once = jnp.logical_and(jnp.logical_not(mine), beside)
+
+    @pl.when(at_once)
+    def _():
+        each_send((1, 2), start_send)
+        each_send((0,), start_send)
+
     lam_copy = remote(lam_own, lam_other, l_sem.at[0], l_sem.at[1], (e, partner))
     lam_copy.start()
-    own_dispatch.start()
-
-    @pl.when(mine)
-    def _():
-        for which in range(3):
-            own_copy(which).start()
+    xbuf[t, e] = slot_ref[pl.ds(pl.multiple_of(e * capacity, capacity), capacity), :]
 
     for copy in weight_copies[:3]:
         copy.wait()
@@ -454,6 +499,47 @@
             def _():
                 pair_out[v, :own_rows, :] = block
 
+    cross_copy.wait_recv()
+    sent_rows = ext_in[:, :model]
+    sent_mix = ext_in[:, model:]
+    taken = (sent_mix[:, :half_slots].astype(jnp.float32) > 0.0).astype(jnp.float32)
+    rel_slots[...] = lax.dot_general(
+        taken.astype(jnp.bfloat16),
+        sent_rows,
+        (((0,), (0,)), ((), ())),
+        preferred_element_type=jnp.float32,
+    ).astype(jnp.bfloat16)
+
+    def pass_on(j):
+        to = lax.rem(place_me + j, half_count)
+        rows = pl.ds(pl.multiple_of(to * capacity, capacity), capacity)
+        return remote(
+            rel_slots.at[rows],
+            xbuf.at[t, across],
+            k_send.at[to],
+            d_recv.at[across],
+            (near_first + to, t),
+        )
+
+    def start_pass(j, carry):
+        pass_on(j).start()
+        return carry
+
+    lax.fori_loop(1, half_count, start_pass, 0)
+    xbuf[t, across] = rel_slots[
+        pl.ds(pl.multiple_of(place_me * capacity, capacity), capacity), :
+    ]
+
+    @pl.when(jnp.logical_not(at_once))
+    def _():
+        each_send((1, 2), start_send)
+        each_send((0,), start_send)
+
+    @pl.when(mine)
+    def _():
+        for which in range(3):
+            own_copy(which).start()
+
     def spread(place, source, far):
         if far == 0:
             sends, recvs, where = g_send.at[source, 0], g_recv.at[source, 0], (e, partner)
@@ -463,26 +549,25 @@
             where = (e, there * 2 + c)
         return remote(place, place, sends, recvs, where)
 
+    def hand_out(source):
+        place = xbuf.at[t, source]
+        for far in range(1, y_count):
+            spread(place, source, far).start()
+        spread(place, source, 0).start()
+
+    hand_out(e)
+    hand_out(across)
+
     def arrive_slots(j, carry):
-        source = lax.rem(e + j, ep_count)
-        place = xbuf.at[t, source]
-
-        @pl.when(source == e)
-        def _():
-            own_dispatch.wait()
-
-        @pl.when(source != e)
-        def _():
+        for source in (near(j), lax.rem(near(j) + half_count, ep_count)):
+            place = xbuf.at[t, source]
             remote(
                 place, place, d_send.at[source], d_recv.at[source], (e, partner)
             ).wait_recv()
-
-        for far in range(1, y_count):
-            spread(place, source, far).start()
-        spread(place, source, 0).start()
-        return carry
-
-    lax.fori_loop(0, ep_count, arrive_slots, 0)
+            hand_out(source)
+        return carry
+
+    lax.fori_loop(1, half_count, arrive_slots, 0)
 
     def relay(source, far, core):
         from_y = lax.rem(y + y_count - far, y_count)
@@ -492,14 +577,14 @@
         )
 
     def arrive_far(j, carry):
-        source = lax.rem(e + j, ep_count)
-        for far in range(1, y_count):
-            from_y = lax.rem(y + y_count - far, y_count)
-            spread(xbuf.at[from_y * 2 + c, source], source, far).wait_recv()
-            relay(source, far, c).start()
-        return carry
-
-    lax.fori_loop(0, ep_count, arrive_far, 0)
+        for source in (near(j), lax.rem(near(j) + half_count, ep_count)):
+            for far in range(1, y_count):
+                from_y = lax.rem(y + y_count - far, y_count)
+                spread(xbuf.at[from_y * 2 + c, source], source, far).wait_recv()
+                relay(source, far, c).start()
+        return carry
+
+    lax.fori_loop(0, half_count, arrive_far, 0)
 
     def arrive_relay(j, carry):
         source = lax.rem(e + j, ep_count)
@@ -573,25 +658,32 @@
 
     def give_back(target):
         return remote(
-            ret_out.at[target], ret_in.at[e], v_send.at[target], v_recv.at[e], (target, t)
-        )
-
-    own_back = pltpu.make_async_copy(ret_out.at[e], ret_in.at[e], v_recv.at[e])
-
-    for step in range(1, y_count):
-        far_copy(step).wait_recv()
-    expert_sum = pair_own[y].astype(jnp.float32)
-    for step in range(1, y_count):
-        expert_sum = expert_sum + far_in[step - 1].astype(jnp.float32)
-    shared_sum[...] = expert_sum[:own_rows]
-    ret_out[...] = expert_sum[own_rows:].astype(jnp.bfloat16).reshape(ret_out.shape)
-
-    def start_back(j, carry):
-        give_back(lax.rem(e + 1 + j, ep_count)).start()
-        return carry
-
-    lax.fori_loop(0, ep_count - 1, start_back, 0)
-    own_back.start()
+            ret_out.at[target], ret_in.at[place_me], v_send.at[target], v_recv.at[place_me], (target, t)
+        )
+
+    def give_relay(target):
+        beyond = lax.rem(target + half_count, ep_count)
+        return remote(
+            ret_out.at[beyond], gathered.at[place_me], u_send.at[target], u_recv.at[place_me], (target, t)
+        )
+
+    def finish_experts():
+        for step in range(1, y_count):
+            far_copy(step).wait_recv()
+        expert_sum = pair_own[y].astype(jnp.float32)
+        for step in range(1, y_count):
+            expert_sum = expert_sum + far_in[step - 1].astype(jnp.float32)
+        shared_sum[...] = expert_sum[:own_rows]
+        ret_out[...] = expert_sum[own_rows:].astype(jnp.bfloat16).reshape(ret_out.shape)
+
+        def start_back(j, carry):
+            give_relay(near(j)).start()
+            give_back(near(j)).start()
+            return carry
+
+        lax.fori_loop(1, half_count, start_back, 0)
+        gathered[place_me] = ret_out[across]
+        ret_in[place_me] = ret_out[e]
 
     def arrive_forward(j, carry):
         source = lax.rem(e + j, ep_count)
@@ -608,7 +700,7 @@
 
     lax.fori_loop(0, ep_count, arrive_forward, 0)
     lam_copy.wait()
-    small_copies[4].wait()
+    small_copies[6].wait()
 
     lam = jnp.where(mine, lam_own[...], lam_other[...])[0:1, 0:1]
     gain = gain_ref[...]
@@ -629,15 +721,10 @@
     def back_own(v):
         return pltpu.make_async_copy(obuf.at[e, v], back_place(v), o_recv.at[h_me, v, c])
 
-    pair_count = ep_count // 2
-    pair_me = e // 2
-
-    def attend(j, carry):
-        v = lax.rem(y + 1 + j // pair_count, y_count)
-        at = lax.rem(pair_me + pair_count // 2 + lax.rem(j, pair_count), pair_count)
+    def attend(v, at, first):
         targets = (at * 2, at * 2 + 1)
 
-        @pl.when(j < pair_count)
+        @pl.when(first)
         def _():
             for target in targets:
                 arrived(0, target)
@@ -676,9 +763,43 @@
             def _():
                 back_own(v).start()
 
-        return carry
-
-    lax.fori_loop(0, pair_count * y_count, attend, 0)
+    pair_first = s_me * near_pairs
+
+    def beyond_pair(k):
+        return (1 - s_me) * (pair_count - 1 - k) + s_me * k
+
+    def near_pair(k):
+        return pair_first + lax.rem(pair_me + k, near_pairs)
+
+    def attend_rows(j, carry):
+        v = lax.rem(y + 1 + j, y_count)
+        attend(v, beyond_pair(0), j == 0)
+        for k in range(near_pairs):
+            attend(v, near_pair(k), j == 0)
+        pl.when(j == 0)(finish_experts)
+        for k in range(1, near_pairs):
+            attend(v, beyond_pair(k), j == 0)
+        return carry
+
+    lax.fori_loop(0, y_count, attend_rows, 0)
+
+    def arrive_gathered(j, carry):
+        place = gathered.at[lax.rem(place_me + j, half_count)]
+        remote(
+            place, place, u_send.at[near(j)], u_recv.at[lax.rem(place_me + j, half_count)], (e, partner)
+        ).wait_recv()
+        return carry
+
+    lax.fori_loop(1, half_count, arrive_gathered, 0)
+    all_gathered = gathered[...].reshape(half_slots, model)
+    cross_mix = ext_in[:, model:]
+    part = jnp.dot(cross_mix[:, :half_slots], all_gathered, preferred_element_type=jnp.float32)
+    part = part + jnp.dot(
+        cross_mix[:, half_slots:], all_gathered, preferred_element_type=jnp.float32
+    )
+    part_out[...] = part.astype(jnp.bfloat16)
+    part_copy = remote(part_out, part_in, m_sem.at[0], m_sem.at[1], (across, t))
+    part_copy.start()
 
     weight_copies[6].wait()
 
@@ -741,22 +862,21 @@
         block_copy(step).start()
     project(y_count - 1)
 
-    own_back.wait()
-
     def arrive_back(j, carry):
-        source = lax.rem(e + 1 + j, ep_count)
-        place = ret_in.at[source]
-        remote(place, place, v_send.at[source], v_recv.at[source], (e, partner)).wait_recv()
-        return carry
-
-    lax.fori_loop(0, ep_count - 1, arrive_back, 0)
-    mix = mix_ref[pl.ds(pl.multiple_of(t * own_rows, own_rows), own_rows), :]
+        at = lax.rem(place_me + j, half_count)
+        place = ret_in.at[at]
+        remote(place, place, v_send.at[near(j)], v_recv.at[at], (e, partner)).wait_recv()
+        return carry
+
+    lax.fori_loop(1, half_count, arrive_back, 0)
+    wide = mix_ref[own_span, :]
+    mix = jnp.where(s_me == 0, wide[:, :half_slots], wide[:, half_slots:])
     coarse = mix.astype(jnp.bfloat16)
     fine = (mix - coarse.astype(jnp.float32)).astype(jnp.bfloat16)
-    returned = ret_in[...].reshape(slots, ret_in.shape[2])
+    returned = ret_in[...].reshape(half_slots, model)
     combined = jnp.dot(coarse, returned, preferred_element_type=jnp.float32)
     combined = combined + jnp.dot(fine, returned, preferred_element_type=jnp.float32)
-    moe_ref[...] = (shared_sum[...] + combined).astype(jnp.bfloat16)
+    shared_sum[...] = shared_sum[...] + combined
 
     pair_copy(y_count - 1).wait()
     total = (
@@ -767,6 +887,8 @@
         block_copy(step).wait()
         total = total + block_in[step - 1].astype(jnp.float32)
     out_ref[...] = total.astype(jnp.bfloat16)
+    part_copy.wait()
+    moe_ref[...] = (shared_sum[...] + part_in[...].astype(jnp.float32)).astype(jnp.bfloat16)
 
     def end_send(whiches, h, side, own):
         @pl.when(jnp.logical_not(own))
@@ -785,11 +907,6 @@
         for far in range(1, y_count):
             relay(source, far, c).wait_send()
 
-        @pl.when(source != e)
-        def _():
-            dispatch(source).wait_send()
-            give_back(source).wait_send()
-
         for which in (1, 2):
             forward(which, source).wait_send()
 
@@ -801,6 +918,16 @@
         return carry
 
     lax.fori_loop(0, ep_count, end_rest, 0)
+
+    def end_near(j, carry):
+        dispatch(near(j)).wait_send()
+        pass_on(j).wait_send()
+        give_back(near(j)).wait_send()
+        give_relay(near(j)).wait_send()
+        return carry
+
+    lax.fori_loop(1, half_count, end_near, 0)
+    cross_copy.wait_send()
 
 
 def mixer(
@@ -833,23 +960,32 @@
     return pl.pallas_call(
         functools.partial(mixer_kernel, ep_count, tp_count),
         out_shape=(
-            jax.ShapeDtypeStruct((share, model), bf16),
-            jax.ShapeDtypeStruct((own_rows, model), bf16),
+            pltpu.VMEM((share, model), bf16),
+            pltpu.VMEM((own_rows, model), bf16),
         ),
-        in_specs=[pl.BlockSpec(memory_space=pltpu.VMEM)] * 2
-        + [pl.BlockSpec(memory_space=pltpu.SMEM)]
-        + [pl.BlockSpec(memory_space=pltpu.HBM)] * 15,
+        in_specs=[pl.BlockSpec(memory_space=pltpu.SMEM)]
+        + [pl.BlockSpec(memory_space=pltpu.HBM)] * 17,
         out_specs=[pl.BlockSpec(memory_space=pltpu.VMEM)] * 2,
         scratch_shapes=[
+            pltpu.VMEM(tables[0].shape, jnp.float32),
+            pltpu.VMEM(tables[1].shape, jnp.float32),
+            pltpu.VMEM(tables[0].shape[1:], jnp.float32),
+            pltpu.VMEM(tables[0].shape[1:], jnp.float32),
             pltpu.VMEM((1, width), jnp.float32),
             pltpu.VMEM((1, model), jnp.float32),
             pltpu.VMEM((top_count, batch_rows), jnp.int32),
             pltpu.VMEM((top_count, batch_rows), jnp.float32),
             pltpu.VMEM((batch_rows, model), bf16),
-            dma((5,)),
+            dma((7,)),
             pltpu.VMEM((batch_rows, model), bf16),
             pltpu.VMEM((slots, model), bf16),
             pltpu.VMEM((batch_rows, slots), jnp.float32),
+            pltpu.VMEM((own_rows, model + slots), bf16),
+            pltpu.VMEM((own_rows, model + slots), bf16),
+            pltpu.VMEM((slots // 2, model), bf16),
+            pltpu.VMEM((ep_count // 2, capacity, model), bf16),
+            pltpu.VMEM((own_rows, model), bf16),
+            pltpu.VMEM((own_rows, model), bf16),
             pltpu.VMEM((3,) + sequence[0].shape, bf16),
             pltpu.VMEM((3, head_count, 2, half, width), bf16),
             dma((3,)),
@@ -868,10 +1004,15 @@
             pltpu.VMEM((max(1, y_count - 1), own_rows + slots, model), bf16),
             pltpu.VMEM((own_rows, model), jnp.float32),
             pltpu.VMEM((ep_count, capacity, model), bf16),
-            pltpu.VMEM((ep_count, capacity, model), bf16),
+            pltpu.VMEM((ep_count // 2, capacity, model), bf16),
             dma((7,)),
             dma((ep_count,)),
             dma((ep_count,)),
+            dma((2,)),
+            dma((ep_count // 2,)),
+            dma((ep_count,)),
+            dma((ep_count // 2,)),
+            dma((2,)),
             dma((ep_count, y_count)),
             dma((ep_count, y_count)),
             dma((ep_count, max(1, y_count - 1))),
@@ -907,12 +1048,12 @@
             dma((max(1, y_count - 1),)),
         ],
         compiler_params=pltpu.CompilerParams(
-            has_side_effects=True, vmem_limit_bytes=67043328, collective_id=0
+            has_side_effects=True, vmem_limit_bytes=62000000, collective_id=0
         ),
         name="mixer",
     )(
+        lambdas,
         *tables,
-        lambdas,
         head_gain[None, :],
         moe_gain[None, :],
         jnp.transpose(routes),
@@ -956,9 +1097,9 @@
     local_experts = expert_gate.shape[0]
     expert_count = local_experts * ep_count
     capacity = (2 * own_rows * top_count + expert_count - 1) // expert_count
-    one_head_each = ep_count == 2 * head_count and tp_count % 2 == 0 and local_experts == 1 and ep_count % 4 == 0
+    one_head_each = ep_count == 2 * head_count and tp_count % 2 == 0 and local_experts == 1 and ep_count % 4 == 0 and expert_count * capacity % 128 == 0
     if one_head_each:
-        tables = rotation_tables(positions, head_dim)
+        tables = rotation_tables(query_rows, ep_count, head_dim)
         sequence = (queries, key_rows, value_rows)
         weights = (expert_gate, expert_up, expert_down, shared_gate, shared_up, shared_down)
         return mixer(

time: 97.8 us -> 76.7 us (0.78)
  the two profiles are of different devices: /device:TPU:0 before, /device:TPU:18 now
where the time goes in v2:
time: 76.7 us; the launch traced here: 76.1 us
  Pallas kernels  74.1 us (97%)
  local copies, waits for them, and re-layouts  1.36 us (2%)
    pallas_call x1, Pallas kernels, mixer(): pl.pallas_call(functools.partial(mixer_kernel, ep_count, tp_count), out_s...  74.1 us

profile of v2, /device:TPU:18, one launch (start us, length us, event | category | flops | bytes accessed | tf_op | source)
XLA Modules:
  0.0 76.1 jit_solution(5044018245773494197)
XLA Ops:
  0.6 74.1 %mixer.1 = (bf16[64,2048]{1,0:T(8,128)(2,1)S(1)}, bf16[32,2048]{1,0:T(8,128)(2,1)S(1)}) custom-call(f32[4]{0:T(128)} %lam_ref.1, f32[2,256,128]{2,1,0:T(8,128)} %constant.4.clone.turn_hbm, f32[2,8,128]{2,1,0:T(8,128)} %constant.5.clone.base_hbm, f32[1,256]{1,0:T(1,128)} %bitcast.5, f32[1,2048]{1,0:T(1,128)} %bitcast.4, s32[2,128]{1,0:T(2,128)} %bitcast.6, ...), custom_call_target="tpu_custom_call" | custom-call | tf_op jit(solution)/shard_map/mixer/pallas_call | solution.py:960
  74.7 0.7 copy.22
  75.4 0.7 copy.23

commit v3 on v2

--- a/solution.py
+++ b/solution.py
@@ -137,7 +137,7 @@
 def mixer_kernel(
     ep_count,
     tp_count,
-    lam_ref,
+    lam_hbm,
     turn_hbm,
     base_hbm,
     gain_hbm,
@@ -157,6 +157,7 @@
     sdown_hbm,
     out_ref,
     moe_ref,
+    lam_ref,
     turn_ref,
     base_ref,
     cos_ref,
@@ -281,6 +282,7 @@
                 (routes_hbm, routes_ref),
                 (scale_hbm, scale_ref),
                 (mgain_hbm, mgain_ref),
+                (lam_hbm, lam_ref),
                 (rows_hbm, rows_ref),
                 (base_hbm, base_ref),
                 (turn_hbm, turn_ref),
@@ -349,7 +351,7 @@
     def near(j):
         return near_first + lax.rem(place_me + j, half_count)
 
-    for copy in small_copies[:4]:
+    for copy in small_copies[:5]:
         copy.wait()
     widened = rows_ref[...].astype(jnp.float32)
     mean_square = jnp.mean(widened * widened, axis=-1, keepdims=True)
@@ -374,7 +376,11 @@
     ).astype(jnp.bfloat16)
     mixing = sum(scale_ref[k : k + 1, :] * chosen[k] for k in range(len(chosen)))
     mix_ref[...] = jnp.transpose(mixing)
-    lam_own[...] = jnp.full(lam_own.shape, lam_ref[h_me], jnp.float32)
+    head_at = lax.broadcasted_iota(jnp.int32, lam_ref.shape, 1)
+    lam_mine = jnp.sum(
+        jnp.where(head_at == h_me, lam_ref[...], 0.0), axis=1, keepdims=True
+    )
+    lam_own[...] = jnp.broadcast_to(lam_mine, lam_own.shape)
 
     def fold(wide):
         return jnp.where(s_me == 0, wide[:, half_slots:], wide[:, :half_slots])
@@ -386,7 +392,7 @@
     ext_out[:, :model] = norm_ref[own_span, :]
     ext_out[:, model:] = jnp.concatenate([away_coarse, away_fine], axis=1)
 
-    for copy in small_copies[4:6]:
+    for copy in small_copies[5:7]:
         copy.wait()
     base_cos, base_sin = base_ref[0, pl.ds(e, 1), :], base_ref[1, pl.ds(e, 1), :]
     cos_ref[...] = base_cos * turn_ref[0] - base_sin * turn_ref[1]
@@ -429,17 +435,18 @@
     for copy in weight_copies:
         copy.start()
 
-    def dispatch(target):
+    def dispatch(j):
+        target, at = near(j), half_count - j
         rows = pl.ds(pl.multiple_of(target * capacity, capacity), capacity)
         return remote(
-            slot_ref.at[rows], xbuf.at[t, e], d_send.at[target], d_recv.at[e], (target, t)
+            slot_ref.at[rows], xbuf.at[t, at], d_send.at[target], d_recv.at[at], (target, t)
         )
 
     cross_copy = remote(ext_out, ext_in, c_sem.at[0], c_sem.at[1], (across, t))
     cross_copy.start()
 
     def start_dispatch(j, carry):
-        dispatch(near(j)).start()
+        dispatch(j).start()
         return carry
 
     lax.fori_loop(1, half_count, start_dispatch, 0)
@@ -476,7 +483,50 @@
 
     lam_copy = remote(lam_own, lam_other, l_sem.at[0], l_sem.at[1], (e, partner))
     lam_copy.start()
-    xbuf[t, e] = slot_ref[pl.ds(pl.multiple_of(e * capacity, capacity), capacity), :]
+    xbuf[t, 0] = slot_ref[pl.ds(pl.multiple_of(e * capacity, capacity), capacity), :]
+
+    def spread(place, source, far):
+        if far == 0:
+            sends, recvs, where = g_send.at[source, 0], g_recv.at[source, 0], (e, partner)
+        else:
+            there = lax.rem(y + far, y_count)
+            sends, recvs = g_send.at[source, far], g_recv.at[source, far]
+            where = (e, there * 2 + c)
+        return remote(place, place, sends, recvs, where)
+
+    def hand_out(source):
+        place = xbuf.at[t, source]
+        for far in range(1, y_count):
+            spread(place, source, far).start()
+        spread(place, source, 0).start()
+
+    def relay(source, far, core):
+        from_y = lax.rem(y + y_count - far, y_count)
+        place = xbuf.at[from_y * 2 + core, source]
+        return remote(
+            place, place, h_send.at[source, far - 1], h_recv.at[source, far - 1], (e, partner)
+        )
+
+    def arrive_slots(at, carry):
+        place = xbuf.at[t, at]
+        remote(place, place, d_send.at[at], d_recv.at[at], (e, partner)).wait_recv()
+        hand_out(at)
+        return carry
+
+    def arrive_far(source, carry):
+        for far in range(1, y_count):
+            from_y = lax.rem(y + y_count - far, y_count)
+            spread(xbuf.at[from_y * 2 + c, source], source, far).wait_recv()
+            relay(source, far, c).start()
+        return carry
+
+    def arrive_relay(source, carry):
+        spread(xbuf.at[partner, source], source, 0).wait_recv()
+        for far in range(1, y_count):
+            relay(source, far, 1 - c).wait_recv()
+        return carry
+
+    hand_out(0)
 
     for copy in weight_copies[:3]:
         copy.wait()
@@ -499,6 +549,7 @@
             def _():
                 pair_out[v, :own_rows, :] = block
 
+    lax.fori_loop(1, half_count, arrive_slots, 0)
     cross_copy.wait_recv()
     sent_rows = ext_in[:, :model]
     sent_mix = ext_in[:, model:]
@@ -511,13 +562,13 @@
     ).astype(jnp.bfloat16)
 
     def pass_on(j):
-        to = lax.rem(place_me + j, half_count)
+        to, at = lax.rem(place_me + j, half_count), half_count + (half_count - j)
         rows = pl.ds(pl.multiple_of(to * capacity, capacity), capacity)
         return remote(
             rel_slots.at[rows],
-            xbuf.at[t, across],
+            xbuf.at[t, at],
             k_send.at[to],
-            d_recv.at[across],
+            d_recv.at[at],
             (near_first + to, t),
         )
 
@@ -526,7 +577,7 @@
         return carry
 
     lax.fori_loop(1, half_count, start_pass, 0)
-    xbuf[t, across] = rel_slots[
+    xbuf[t, half_count] = rel_slots[
         pl.ds(pl.multiple_of(place_me * capacity, capacity), capacity), :
     ]
 
@@ -540,98 +591,93 @@
         for which in range(3):
             own_copy(which).start()
 
-    def spread(place, source, far):
-        if far == 0:
-            sends, recvs, where = g_send.at[source, 0], g_recv.at[source, 0], (e, partner)
-        else:
-            there = lax.rem(y + far, y_count)
-            sends, recvs = g_send.at[source, far], g_recv.at[source, far]
-            where = (e, there * 2 + c)
-        return remote(place, place, sends, recvs, where)
-
-    def hand_out(source):
-        place = xbuf.at[t, source]
-        for far in range(1, y_count):
-            spread(place, source, far).start()
-        spread(place, source, 0).start()
-
-    hand_out(e)
-    hand_out(across)
-
-    def arrive_slots(j, carry):
-        for source in (near(j), lax.rem(near(j) + half_count, ep_count)):
-            place = xbuf.at[t, source]
-            remote(
-                place, place, d_send.at[source], d_recv.at[source], (e, partner)
-            ).wait_recv()
-            hand_out(source)
-        return carry
-
-    lax.fori_loop(1, half_count, arrive_slots, 0)
-
-    def relay(source, far, core):
-        from_y = lax.rem(y + y_count - far, y_count)
-        place = xbuf.at[from_y * 2 + core, source]
-        return remote(
-            place, place, h_send.at[source, far - 1], h_recv.at[source, far - 1], (e, partner)
-        )
-
-    def arrive_far(j, carry):
-        for source in (near(j), lax.rem(near(j) + half_count, ep_count)):
-            for far in range(1, y_count):
-                from_y = lax.rem(y + y_count - far, y_count)
-                spread(xbuf.at[from_y * 2 + c, source], source, far).wait_recv()
-                relay(source, far, c).start()
-        return carry
-
+    hand_out(half_count)
     lax.fori_loop(0, half_count, arrive_far, 0)
-
-    def arrive_relay(j, carry):
-        source = lax.rem(e + j, ep_count)
-        spread(xbuf.at[partner, source], source, 0).wait_recv()
-        for far in range(1, y_count):
-            relay(source, far, 1 - c).wait_recv()
-        return carry
-
-    lax.fori_loop(0, ep_count, arrive_relay, 0)
-
-    for copy in weight_copies[3:6]:
-        copy.wait()
-    rows_in = xbuf[...].reshape(tp_count * slots, xbuf.shape[3])
-    gate_part = jnp.dot(rows_in, gate_ref[...], preferred_element_type=jnp.float32)
-    up_part = jnp.dot(rows_in, up_ref[...], preferred_element_type=jnp.float32)
-    hidden[...] = (
-        (gate_part / (1.0 + jnp.exp(-gate_part)) * up_part).astype(jnp.bfloat16)
-    ).reshape(hidden.shape)
-
-    def down_part(core, into):
+    lax.fori_loop(half_count + 1, ep_count, arrive_slots, 0)
+
+    def part_rows(part):
+        first = own_rows + part * half_slots
+        return slice(first if part else 0, first + half_slots)
+
+    def down_part(core, into, part):
         rows = jnp.concatenate([hidden[v * 2 + core] for v in range(y_count)], axis=0)
         product = jnp.dot(rows, down_ref[...], preferred_element_type=jnp.float32)
         product = product.astype(jnp.bfloat16)
+        first = own_rows + part * half_slots
         for v in range(y_count):
-            into[v, own_rows:, :] = product[v * slots : (v + 1) * slots]
-
-    down_part(1 - c, pair_out)
-    near_copy = remote(pair_out, pair_in, p_sem.at[0], p_sem.at[1], (e, partner))
-    near_copy.start()
-    down_part(c, pair_own)
-    near_copy.wait()
-    pair_own[...] = (
-        pair_own[...].astype(jnp.float32) + pair_in[...].astype(jnp.float32)
-    ).astype(jnp.bfloat16)
-
-    def far_copy(step):
+            into[v, first : first + half_slots, :] = product[v * half_slots : (v + 1) * half_slots]
+
+    def far_copy(step, part):
         target = lax.rem(y + step, y_count)
+        rows = part_rows(part)
         return remote(
-            pair_own.at[target],
-            far_in.at[step - 1],
-            y_send.at[step - 1],
-            y_recv.at[step - 1],
+            pair_own.at[target, rows],
+            far_in.at[step - 1, rows],
+            y_send.at[part, step - 1],
+            y_recv.at[part, step - 1],
             (e, target * 2 + c),
         )
 
-    for step in range(1, y_count):
-        far_copy(step).start()
+    for part in range(2):
+        first, last = part * half_count, (part + 1) * half_count
+        if part > 0:
+            lax.fori_loop(first, last, arrive_far, 0)
+        lax.fori_loop(first, last, arrive_relay, 0)
+        if part == 0:
+            for copy in weight_copies[3:6]:
+                copy.wait()
+        rows_in = xbuf[:, first:last].reshape(tp_count * half_slots, model)
+        gate_part = jnp.dot(rows_in, gate_ref[...], preferred_element_type=jnp.float32)
+        up_part = jnp.dot(rows_in, up_ref[...], preferred_element_type=jnp.float32)
+        hidden[...] = (
+            (gate_part / (1.0 + jnp.exp(-gate_part)) * up_part).astype(jnp.bfloat16)
+        ).reshape(hidden.shape)
+        down_part(1 - c, pair_out, part)
+        rows = part_rows(part)
+        near_copy = remote(
+            pair_out.at[:, rows], pair_in.at[:, rows], p_sem.at[part, 0], p_sem.at[part, 1], (e, partner)
+        )
+        near_copy.start()
+        down_part(c, pair_own, part)
+        near_copy.wait()
+        pair_own[:, rows] = (
+            pair_own[:, rows].astype(jnp.float32) + pair_in[:, rows].astype(jnp.float32)
+        ).astype(jnp.bfloat16)
+        for step in range(1, y_count):
+            far_copy(step, part).start()
+
+    def give_back(j):
+        return remote(
+            ret_out.at[j], ret_in.at[place_me], v_send.at[j], v_recv.at[place_me], (near(j), t)
+        )
+
+    def give_relay(j):
+        return remote(
+            ret_out.at[half_count + j], gathered.at[place_me], u_send.at[j], u_recv.at[place_me], (near(j), t)
+        )
+
+    def finish_experts(part):
+        rows = part_rows(part)
+        for step in range(1, y_count):
+            far_copy(step, part).wait_recv()
+        expert_sum = pair_own[y, rows].astype(jnp.float32)
+        for step in range(1, y_count):
+            expert_sum = expert_sum + far_in[step - 1, rows].astype(jnp.float32)
+        if part == 0:
+            shared_sum[...] = expert_sum[:own_rows]
+            expert_sum = expert_sum[own_rows:]
+        first, last = part * half_count, (part + 1) * half_count
+        ret_out[first:last] = expert_sum.astype(jnp.bfloat16).reshape(
+            (half_count,) + ret_out.shape[1:]
+        )
+        give = (give_back, give_relay)[part]
+
+        def start_give(j, carry):
+            give(j).start()
+            return carry
+
+        lax.fori_loop(1, half_count, start_give, 0)
+        (ret_in, gathered)[part][place_me] = ret_out[first]
 
     def arrived(which, source):
         own = jnp.logical_and(source == e, mine)
@@ -655,35 +701,6 @@
         return carry
 
     lax.fori_loop(0, ep_count, arrive, 0)
-
-    def give_back(target):
-        return remote(
-            ret_out.at[target], ret_in.at[place_me], v_send.at[target], v_recv.at[place_me], (target, t)
-        )
-
-    def give_relay(target):
-        beyond = lax.rem(target + half_count, ep_count)
-        return remote(
-            ret_out.at[beyond], gathered.at[place_me], u_send.at[target], u_recv.at[place_me], (target, t)
-        )
-
-    def finish_experts():
-        for step in range(1, y_count):
-            far_copy(step).wait_recv()
-        expert_sum = pair_own[y].astype(jnp.float32)
-        for step in range(1, y_count):
-            expert_sum = expert_sum + far_in[step - 1].astype(jnp.float32)
-        shared_sum[...] = expert_sum[:own_rows]
-        ret_out[...] = expert_sum[own_rows:].astype(jnp.bfloat16).reshape(ret_out.shape)
-
-        def start_back(j, carry):
-            give_relay(near(j)).start()
-            give_back(near(j)).start()
-            return carry
-
-        lax.fori_loop(1, half_count, start_back, 0)
-        gathered[place_me] = ret_out[across]
-        ret_in[place_me] = ret_out[e]
 
     def arrive_forward(j, carry):
         source = lax.rem(e + j, ep_count)
@@ -700,7 +717,7 @@
 
     lax.fori_loop(0, ep_count, arrive_forward, 0)
     lam_copy.wait()
-    small_copies[6].wait()
+    small_copies[7].wait()
 
     lam = jnp.where(mine, lam_own[...], lam_other[...])[0:1, 0:1]
     gain = gain_ref[...]
@@ -721,16 +738,11 @@
     def back_own(v):
         return pltpu.make_async_copy(obuf.at[e, v], back_place(v), o_recv.at[h_me, v, c])
 
-    def attend(v, at, first):
-        targets = (at * 2, at * 2 + 1)
-
-        @pl.when(first)
-        def _():
-            for target in targets:
-                arrived(0, target)
-
-        rows = pl.ds(pl.multiple_of(v * share, share), share)
-        block = jnp.concatenate([qbuf[target, rows, :] for target in targets], axis=0)
+    def attend(pieces):
+        def rows_of(v):
+            return pl.ds(pl.multiple_of(v * share, share), share)
+
+        block = jnp.concatenate([qbuf[target, rows_of(v), :] for target, v in pieces], axis=0)
         ratios = []
         for m in range(2):
             columns = slice(m * head_dim, (m + 1) * head_dim)
@@ -750,9 +762,9 @@
         mixed = ratios[0] - lam * ratios[1]
         mean_square = jnp.mean(mixed * mixed, axis=-1, keepdims=True)
         done = (mixed * lax.rsqrt(mean_square + head_eps) * gain).astype(jnp.bfloat16)
-        for k, target in enumerate(targets):
+        for k, (target, v) in enumerate(pieces):
             obuf[target, v] = done[k * share : (k + 1) * share]
-        for target in targets:
+        for target, v in pieces:
             own = jnp.logical_and(target == e, mine)
 
             @pl.when(jnp.logical_not(own))
@@ -771,35 +783,54 @@
     def near_pair(k):
         return pair_first + lax.rem(pair_me + k, near_pairs)
 
-    def attend_rows(j, carry):
-        v = lax.rem(y + 1 + j, y_count)
-        attend(v, beyond_pair(0), j == 0)
-        for k in range(near_pairs):
-            attend(v, near_pair(k), j == 0)
-        pl.when(j == 0)(finish_experts)
-        for k in range(1, near_pairs):
-            attend(v, beyond_pair(k), j == 0)
-        return carry
-
-    lax.fori_loop(0, y_count, attend_rows, 0)
+    v_order = [lax.rem(y + 1 + j, y_count) for j in range(y_count)]
+
+    def await_queries(pair):
+        for k in range(2):
+            arrived(0, pair * 2 + k)
+
+    def both(pair, v):
+        return [(pair * 2 + k, v) for k in range(2)]
+
+    def attend_near(v):
+        attend([piece for k in range(near_pairs) for piece in both(near_pair(k), v)])
+
+    def attend_beyond(k):
+        await_queries(beyond_pair(k))
+        attend([piece for v in v_order for piece in both(beyond_pair(k), v)])
+
+    for k in range(near_pairs):
+        await_queries(near_pair(k))
+    attend_near(v_order[0])
+    finish_experts(0)
+    attend_beyond(0)
+    finish_experts(1)
+    for v in v_order[1:]:
+        attend_near(v)
+    for k in range(1, near_pairs):
+        attend_beyond(k)
 
     def arrive_gathered(j, carry):
         place = gathered.at[lax.rem(place_me + j, half_count)]
         remote(
-            place, place, u_send.at[near(j)], u_recv.at[lax.rem(place_me + j, half_count)], (e, partner)
+            place, place, u_send.at[j], u_recv.at[lax.rem(place_me + j, half_count)], (e, partner)
         ).wait_recv()
         return carry
 
-    lax.fori_loop(1, half_count, arrive_gathered, 0)
-    all_gathered = gathered[...].reshape(half_slots, model)
-    cross_mix = ext_in[:, model:]
-    part = jnp.dot(cross_mix[:, :half_slots], all_gathered, preferred_element_type=jnp.float32)
-    part = part + jnp.dot(
-        cross_mix[:, half_slots:], all_gathered, preferred_element_type=jnp.float32
-    )
-    part_out[...] = part.astype(jnp.bfloat16)
     part_copy = remote(part_out, part_in, m_sem.at[0], m_sem.at[1], (across, t))
-    part_copy.start()
+
+    def mix_across():
+        lax.fori_loop(1, half_count, arrive_gathered, 0)
+        all_gathered = gathered[...].reshape(half_slots, model)
+        cross_mix = ext_in[:, model:]
+        part = jnp.dot(cross_mix[:, :half_slots], all_gathered, preferred_element_type=jnp.float32)
+        part = part + jnp.dot(
+            cross_mix[:, half_slots:], all_gathered, preferred_element_type=jnp.float32
+        )
+        part_out[...] = part.astype(jnp.bfloat16)
+        part_copy.start()
+
+    pl.when(beside)(mix_across)
 
     weight_copies[6].wait()
 
@@ -860,12 +891,13 @@
             kept[step - 1].astype(jnp.float32) + sum_in[step - 1].astype(jnp.float32)
         ).astype(jnp.bfloat16)
         block_copy(step).start()
+    pl.when(jnp.logical_not(beside))(mix_across)
     project(y_count - 1)
 
     def arrive_back(j, carry):
         at = lax.rem(place_me + j, half_count)
         place = ret_in.at[at]
-        remote(place, place, v_send.at[near(j)], v_recv.at[at], (e, partner)).wait_recv()
+        remote(place, place, v_send.at[j], v_recv.at[at], (e, partner)).wait_recv()
         return carry
 
     lax.fori_loop(1, half_count, arrive_back, 0)
@@ -899,7 +931,8 @@
     each_send((0, 1, 2), end_send)
 
     for step in range(1, y_count):
-        far_copy(step).wait_send()
+        for part in range(2):
+            far_copy(step, part).wait_send()
 
     def end_rest(source, carry):
         for far in range(y_count):
@@ -920,10 +953,10 @@
     lax.fori_loop(0, ep_count, end_rest, 0)
 
     def end_near(j, carry):
-        dispatch(near(j)).wait_send()
+        dispatch(j).wait_send()
         pass_on(j).wait_send()
-        give_back(near(j)).wait_send()
-        give_relay(near(j)).wait_send()
+        give_back(j).wait_send()
+        give_relay(j).wait_send()
         return carry
 
     lax.fori_loop(1, half_count, end_near, 0)
@@ -963,10 +996,10 @@
             pltpu.VMEM((share, model), bf16),
             pltpu.VMEM((own_rows, model), bf16),
         ),
-        in_specs=[pl.BlockSpec(memory_space=pltpu.SMEM)]
-        + [pl.BlockSpec(memory_space=pltpu.HBM)] * 17,
+        in_specs=[pl.BlockSpec(memory_space=pltpu.HBM)] * 18,
         out_specs=[pl.BlockSpec(memory_space=pltpu.VMEM)] * 2,
         scratch_shapes=[
+            pltpu.VMEM((1, head_count), jnp.float32),
             pltpu.VMEM(tables[0].shape, jnp.float32),
             pltpu.VMEM(tables[1].shape, jnp.float32),
             pltpu.VMEM(tables[0].shape[1:], jnp.float32),
@@ -976,7 +1009,7 @@
             pltpu.VMEM((top_count, batch_rows), jnp.int32),
             pltpu.VMEM((top_count, batch_rows), jnp.float32),
             pltpu.VMEM((batch_rows, model), bf16),
-            dma((7,)),
+            dma((8,)),
             pltpu.VMEM((batch_rows, model), bf16),
             pltpu.VMEM((slots, model), bf16),
             pltpu.VMEM((batch_rows, slots), jnp.float32),
@@ -997,7 +1030,7 @@
             pltpu.VMEM((model, shared_width), bf16),
             pltpu.VMEM((shared_width, model), bf16),
             pltpu.VMEM((tp_count, ep_count, capacity, model), bf16),
-            pltpu.VMEM((tp_count, slots, hidden_width), bf16),
+            pltpu.VMEM((tp_count, slots // 2, hidden_width), bf16),
             pltpu.VMEM((y_count, own_rows + slots, model), bf16),
             pltpu.VMEM((y_count, own_rows + slots, model), bf16),
             pltpu.VMEM((y_count, own_rows + slots, model), bf16),
@@ -1017,9 +1050,9 @@
             dma((ep_count, y_count)),
             dma((ep_count, max(1, y_count - 1))),
             dma((ep_count, max(1, y_count - 1))),
-            dma((2,)),
-            dma((max(1, y_count - 1),)),
-            dma((max(1, y_count - 1),)),
+            dma((2, 2)),
+            dma((2, max(1, y_count - 1))),
+            dma((2, max(1, y_count - 1))),
             dma((ep_count,)),
             dma((ep_count,)),
             pltpu.VMEM((ep_count, half, width), bf16),
@@ -1052,7 +1085,7 @@
         ),
         name="mixer",
     )(
-        lambdas,
+        lambdas[None, :],
         *tables,
         head_gain[None, :],
         moe_gain[None, :],

time: 76.7 us -> 71.8 us (0.936)
  Pallas kernels: 74.1 us -> 69.6 us
    pallas_call x1, Pallas kernels: 74.1 us -> 69.6 us  [mixer(): pl.pallas_call(functools.partial(mixer_kernel, ep_count, tp_count), out_s...]
where the time goes in v3:
time: 71.8 us; the launch traced here: 71.6 us
  Pallas kernels  69.6 us (97%)
  local copies, waits for them, and re-layouts  1.36 us (2%)
    pallas_call x1, Pallas kernels, mixer(): pl.pallas_call(functools.partial(mixer_kernel, ep_count, tp_count), out_s...  69.6 us

profile of v3, /device:TPU:18, one launch (start us, length us, event | category | flops | bytes accessed | tf_op | source)
XLA Modules:
  0.0 71.6 jit_solution(8276206595736148325)
XLA Ops:
  0.6 69.6 %mixer.1 = (bf16[64,2048]{1,0:T(8,128)(2,1)S(1)}, bf16[32,2048]{1,0:T(8,128)(2,1)S(1)}) custom-call(f32[1,4]{1,0:T(1,128)} %bitcast.9, f32[2,256,128]{2,1,0:T(8,128)} %constant.4.clone.turn_hbm, f32[2,8,128]{2,1,0:T(8,128)} %constant.5.clone.base_hbm, f32[1,256]{1,0:T(1,128)} %bitcast.6, f32[1,2048]{1,0:T(1,128)} %bitcast.5, s32[2,128]{1,0:T(2,128)} %bitcast.7, ...), custom_call_target="tpu_custom_call" | custom-call | tf_op jit(solution)/shard_map/mixer/pallas_call | solution.py:993
  70.3 0.7 copy.22
  71.0 0.7 copy.23

commit v4 on v3

--- a/solution.py
+++ b/solution.py
@@ -834,8 +834,27 @@
 
     weight_copies[6].wait()
 
-    def pair_copy(at):
-        return remote(sum_out.at[at], sum_in.at[at], r_send.at[at], r_recv.at[at], (e, partner))
+    column_parts = 2
+    part_width = model // column_parts
+
+    def columns_of(part):
+        return slice(part * part_width, (part + 1) * part_width)
+
+    def pair_copy(at, part):
+        columns = columns_of(part)
+        return remote(
+            sum_out.at[at, :, columns],
+            sum_in.at[at, :, columns],
+            r_send.at[at, part],
+            r_recv.at[at, part],
+            (e, partner),
+        )
+
+    def pair_sum(at, part):
+        pair_copy(at, part).wait()
+        columns = columns_of(part)
+        mine_part = kept[at, :, columns].astype(jnp.float32)
+        return (mine_part + sum_in[at, :, columns].astype(jnp.float32)).astype(jnp.bfloat16)
 
     def project(at):
         v = lax.rem(y + 1 + at, y_count)
@@ -860,37 +879,41 @@
             return carry
 
         lax.fori_loop(0, head_count, arrive_heads, 0)
-        total = None
-        for h in range(head_count):
-            rows = jnp.concatenate([heads[h, v, 1 - c], heads[h, v, c]], axis=0)
-            term = jnp.dot(
-                rows,
-                proj_ref[h * width : (h + 1) * width, :],
-                preferred_element_type=jnp.float32,
-            )
-            total = term if total is None else total + term
-        total = total.astype(jnp.bfloat16)
-        sum_out[at] = total[:share]
-        kept[at] = total[share:]
-        pair_copy(at).start()
-
-    def block_copy(step):
+        rows = [
+            jnp.concatenate([heads[h, v, 1 - c], heads[h, v, c]], axis=0)
+            for h in range(head_count)
+        ]
+        for part in range(column_parts):
+            columns = columns_of(part)
+            total = None
+            for h in range(head_count):
+                term = jnp.dot(
+                    rows[h],
+                    proj_ref[h * width : (h + 1) * width, columns],
+                    preferred_element_type=jnp.float32,
+                )
+                total = term if total is None else total + term
+            total = total.astype(jnp.bfloat16)
+            sum_out[at, :, columns] = total[:share]
+            kept[at, :, columns] = total[share:]
+            pair_copy(at, part).start()
+
+    def block_copy(step, part):
         target = lax.rem(y + step, y_count)
+        columns = columns_of(part)
         return remote(
-            block_out.at[step - 1],
-            block_in.at[step - 1],
-            b_send.at[step - 1],
-            b_recv.at[step - 1],
+            block_out.at[step - 1, :, columns],
+            block_in.at[step - 1, :, columns],
+            b_send.at[step - 1, part],
+            b_recv.at[step - 1, part],
             (e, target * 2 + c),
         )
 
     for step in range(1, y_count):
         project(step - 1)
-        pair_copy(step - 1).wait()
-        block_out[step - 1] = (
-            kept[step - 1].astype(jnp.float32) + sum_in[step - 1].astype(jnp.float32)
-        ).astype(jnp.bfloat16)
-        block_copy(step).start()
+        for part in range(column_parts):
+            block_out[step - 1, :, columns_of(part)] = pair_sum(step - 1, part)
+            block_copy(step, part).start()
     pl.when(jnp.logical_not(beside))(mix_across)
     project(y_count - 1)
 
@@ -910,15 +933,13 @@
     combined = combined + jnp.dot(fine, returned, preferred_element_type=jnp.float32)
     shared_sum[...] = shared_sum[...] + combined
 
-    pair_copy(y_count - 1).wait()
-    total = (
-        kept[y_count - 1].astype(jnp.float32) + sum_in[y_count - 1].astype(jnp.float32)
-    ).astype(jnp.bfloat16)
-    total = total.astype(jnp.float32)
-    for step in range(1, y_count):
-        block_copy(step).wait()
-        total = total + block_in[step - 1].astype(jnp.float32)
-    out_ref[...] = total.astype(jnp.bfloat16)
+    for part in range(column_parts):
+        columns = columns_of(part)
+        total = pair_sum(y_count - 1, part).astype(jnp.float32)
+        for step in range(1, y_count):
+            block_copy(step, part).wait()
+            total = total + block_in[step - 1, :, columns].astype(jnp.float32)
+        out_ref[:, columns] = total.astype(jnp.bfloat16)
     part_copy.wait()
     moe_ref[...] = (shared_sum[...] + part_in[...].astype(jnp.float32)).astype(jnp.bfloat16)
 
@@ -961,6 +982,29 @@
 
     lax.fori_loop(1, half_count, end_near, 0)
     cross_copy.wait_send()
+
+
+def place_kernel(first_ref, second_ref, first_hbm, second_hbm, sem):
+    copies = [
+        pltpu.make_async_copy(first_ref, first_hbm, sem.at[0]),
+        pltpu.make_async_copy(second_ref, second_hbm, sem.at[1]),
+    ]
+    for copy in copies:
+        copy.start()
+    for copy in copies:
+        copy.wait()
+
+
+def place_results(results):
+    return pl.pallas_call(
+        place_kernel,
+        out_shape=tuple(jax.ShapeDtypeStruct(r.shape, r.dtype) for r in results),
+        in_specs=[pl.BlockSpec(memory_space=pltpu.VMEM)] * 2,
+        out_specs=[pl.BlockSpec(memory_space=pltpu.HBM)] * 2,
+        scratch_shapes=[pltpu.SemaphoreType.DMA((2,))],
+        compiler_params=pltpu.CompilerParams(vmem_limit_bytes=1024 * 1024),
+        name="place",
+    )(*results)
 
 
 def mixer(
@@ -1075,10 +1119,10 @@
             dma((2,)),
             dma((ep_count, y_count)),
             dma((head_count, y_count, 2)),
-            dma((y_count,)),
-            dma((y_count,)),
-            dma((max(1, y_count - 1),)),
-            dma((max(1, y_count - 1),)),
+            dma((y_count, 2)),
+            dma((y_count, 2)),
+            dma((max(1, y_count - 1), 2)),
+            dma((max(1, y_count - 1), 2)),
         ],
         compiler_params=pltpu.CompilerParams(
             has_side_effects=True, vmem_limit_bytes=62000000, collective_id=0
@@ -1135,7 +1179,7 @@
         tables = rotation_tables(query_rows, ep_count, head_dim)
         sequence = (queries, key_rows, value_rows)
         weights = (expert_gate, expert_up, expert_down, shared_gate, shared_up, shared_down)
-        return mixer(
+        return place_results(mixer(
             tables,
             sequence,
             lambdas,
@@ -1146,7 +1190,7 @@
             ep_count,
             tp_count,
             capacity,
-        )
+        ))
     else:
         rot_query = rotate(queries, positions, head_dim)
         rot_keys = rotate(key_rows, positions, head_dim)

time: 71.8 us -> 70.9 us (0.987)
  local copies, waits for them, and re-layouts: 1.36 us -> 0 us
    unnamed x2 -> x0, local copies, waits for them, and re-layouts: 1.36 us -> none
    pallas_call x0 -> x1, Pallas kernels: none -> 0.76 us  [place_results(): pl.pallas_call(place_kernel, out_shape=tuple((jax.ShapeDtypeStruct(r.shap...]
where the time goes in v4:
time: 70.9 us; the launch traced here: 70.7 us
  Pallas kernels  69.9 us (99%)
  between operations  0.81 us (1%)
    pallas_call x1, Pallas kernels, mixer(): pl.pallas_call(functools.partial(mixer_kernel, ep_count, tp_count), out_s...  69.2 us

profile of v4, /device:TPU:18, one launch (start us, length us, event | category | flops | bytes accessed | tf_op | source)
XLA Modules:
  0.0 70.7 jit_solution(3702980446502878979)
XLA Ops:
  0.6 69.2 %mixer.1 = (bf16[64,2048]{1,0:T(8,128)(2,1)S(1)}, bf16[32,2048]{1,0:T(8,128)(2,1)S(1)}) custom-call(f32[1,4]{1,0:T(1,128)} %bitcast.9, f32[2,256,128]{2,1,0:T(8,128)} %constant.4.clone.turn_hbm, f32[2,8,128]{2,1,0:T(8,128)} %constant.5.clone.base_hbm, f32[1,256]{1,0:T(1,128)} %bitcast.6, f32[1,2048]{1,0:T(1,128)} %bitcast.5, s32[2,128]{1,0:T(2,128)} %bitcast.7, ...), custom_call_target="tpu_custom_call" | custom-call | tf_op jit(solution)/shard_map/mixer/pallas_call | solution.py:1037
  69.8 0.8 %place.1 = (bf16[64,2048]{1,0:T(8,128)(2,1)}, bf16[32,2048]{1,0:T(8,128)(2,1)}) custom-call(bf16[64,2048]{1,0:T(8,128)(2,1)S(1)} %get-tuple-element.4.first_ref, bf16[32,2048]{1,0:T(8,128)(2,1)S(1)} %get-tuple-element.5.second_ref), custom_call_target="tpu_custom_call" | custom-call | tf_op jit(solution)/shard_map/place/pallas_call | solution.py:999

commit v5 on v4

--- a/solution.py
+++ b/solution.py
@@ -808,7 +808,9 @@
     for v in v_order[1:]:
         attend_near(v)
     for k in range(1, near_pairs):
-        attend_beyond(k)
+        await_queries(beyond_pair(k))
+        for v in v_order:
+            attend(both(beyond_pair(k), v))
 
     def arrive_gathered(j, carry):
         place = gathered.at[lax.rem(place_me + j, half_count)]

time: 70.9 us -> 70.9 us (level)
  no operation moved by 1% of the time
where the time goes in v5:
time: 70.9 us; the launch traced here: 70.7 us
  Pallas kernels  69.9 us (99%)
  between operations  0.81 us (1%)
    pallas_call x1, Pallas kernels, mixer(): pl.pallas_call(functools.partial(mixer_kernel, ep_count, tp_count), out_s...  69.2 us

profile of v5, /device:TPU:18, one launch (start us, length us, event | category | flops | bytes accessed | tf_op | source)
XLA Modules:
  0.0 70.7 jit_solution(5451380724958728902)
XLA Ops:
  0.6 69.2 %mixer.1 = (bf16[64,2048]{1,0:T(8,128)(2,1)S(1)}, bf16[32,2048]{1,0:T(8,128)(2,1)S(1)}) custom-call(f32[1,4]{1,0:T(1,128)} %bitcast.9, f32[2,256,128]{2,1,0:T(8,128)} %constant.4.clone.turn_hbm, f32[2,8,128]{2,1,0:T(8,128)} %constant.5.clone.base_hbm, f32[1,256]{1,0:T(1,128)} %bitcast.6, f32[1,2048]{1,0:T(1,128)} %bitcast.5, s32[2,128]{1,0:T(2,128)} %bitcast.7, ...), custom_call_target="tpu_custom_call" | custom-call | tf_op jit(solution)/shard_map/mixer/pallas_call | solution.py:1039
  69.8 0.8 %place.1 = (bf16[64,2048]{1,0:T(8,128)(2,1)}, bf16[32,2048]{1,0:T(8,128)(2,1)}) custom-call(bf16[64,2048]{1,0:T(8,128)(2,1)S(1)} %get-tuple-element.4.first_ref, bf16[32,2048]{1,0:T(8,128)(2,1)S(1)} %get-tuple-element.5.second_ref), custom_call_target="tpu_custom_call" | custom-call | tf_op jit(solution)/shard_map/place/pallas_call | solution.py:1001
